TPU v7x, 256 devices: a 4x2x16 block of a 4x16x16 slice. The times are simulated.
256 devices in a mesh: grp: 2 (over y), fs: 32 (over z, core), tp: 4 (over x).
Axes of the slice: x: 4, y: 2, z: 16, core: 2. Of those that a mesh axis runs over, the one named last changes fastest.
The devices are a block of a 4x16x16 slice.
Arguments:
- tokens: bfloat16 [1536, 2048], P(('grp', 'tp')), parts along dimension 0, may hold values from -6 to 6
- norm_gain: float32 [2048], P('fs'), may hold values from 0.1 to 1.9
- up_trained: float32 [2048, 8192], P('fs', 'tp'), may hold values from -0.125 to 0.125
- down_trained: float32 [2048, 8192], P('fs', 'tp'), may hold values from -0.125 to 0.125
Outputs:
- up_serving: bfloat16 [4096, 8192], P('grp', 'fs'), parts along dimension 0
- down_serving: bfloat16 [4096, 8192], P('grp', 'fs'), parts along dimension 0
- prompt_output: bfloat16 [1536, 2048], P(('grp', 'tp'), 'fs'), parts along dimension 0
There are 2 independent parts, one for each index of `grp`. A program takes and returns all parts, laid end to end along the dimension named above; an argument that names none is the same for every part. Nothing has to cross between parts.
All inputs are finite; a program needn't handle non-finite values.
Results may differ from a plain program's by a relative error of at most 0.0074.
Values may be sent and summed in bfloat16 or wider, within the bound.
No kernel may reach another device: no remote copies, remote signals or barrier semaphores. Data moves between devices by JAX's collectives and lax.ppermute only.
A program may use at most 64 MiB of HBM per device.

v0:
```python
import functools

import jax
import jax.numpy as jnp
from jax import lax
from jax.experimental import pallas as pl
from jax.experimental.pallas import tpu as pltpu
from jax.sharding import PartitionSpec as P


epsilon = 1e-06
CORES = 2
PAIR = 2
LANES = 128


def ring(devices, step):
    return [(i, (i + step) % devices) for i in range(devices)]


def across(devices, step):
    return [
        (member * devices + i, (1 - member) * devices + (i + step) % devices)
        for member in range(PAIR)
        for i in range(devices)
    ]


def nt_dot(a, b):
    return lax.dot_general(a, b, (((1,), (1,)), ((), ())), preferred_element_type=jnp.float32)


def partial_sums(out, side, cores, active, down):
    shards, groups, quarter, width = down.shape
    rows, chips = groups * quarter, shards // cores
    head, tail = active[:LANES], active[LANES:]
    none = jnp.zeros_like(tail)
    upper, lower = jnp.concatenate([tail, none]), jnp.concatenate([none, tail])
    weights = down.reshape(chips, cores, rows, width)[:, pl.ds(side, 1)][:, 0]
    out[:, :rows] = nt_dot(weights.reshape(chips * rows, width), head).astype(out.dtype).reshape(chips, rows, LANES)
    packed = nt_dot(weights[:, : rows // 2].reshape(chips * rows // 2, width), upper) + nt_dot(
        weights[:, rows // 2 :].reshape(chips * rows // 2, width), lower
    )
    out[:, rows:] = packed.astype(out.dtype).reshape(chips, rows // 2, LANES)


def feed_forward(cores, where, normed, *refs):
    quarters, (up, down, active, away) = refs[:-4], refs[-4:]
    shards, groups, quarter, width = up.shape
    at, core, member = where[0], where[1], where[2]

    def place(weight, own, left, far_first, far_second, right):
        half = shards // 2
        for step, first, count, piece in (
            (0, 0, shards, own),
            (1, 0, shards, left),
            (2, 0, half, far_first),
            (2, half, half, far_second),
            (3, 0, shards, right),
        ):
            slot = lax.rem(at + step, groups)
            weight[pl.ds(first, count), pl.ds(slot, 1)] = piece[...][:, None]

    for value, mine, other in ((0, up, down), (1, down, up)):

        @pl.when(member == value)
        def _(mine=mine, other=other):
            place(mine, *quarters[:5])
            place(other, *quarters[5:])

    hidden = jnp.dot(
        normed[...], up[...].reshape(shards * groups * quarter, width), preferred_element_type=jnp.float32
    )
    rounded = jnp.square(jnp.maximum(hidden, 0.0)).astype(active.dtype)
    active[...] = rounded
    partial_sums(away, 1 - core, cores, rounded, down)


def own_side(cores, where, active, up, down, up_out, down_out, kept, sems):
    writes = [pltpu.make_async_copy(up, up_out, sems.at[0]), pltpu.make_async_copy(down, down_out, sems.at[1])]
    for write in writes:
        write.start()
    partial_sums(kept, where[1], cores, active[...], down)
    for write in writes:
        write.wait()


def added(a, b):
    return (a.astype(jnp.float32) + b.astype(jnp.float32)).astype(jnp.bfloat16)


def summed_up(arrived, out):
    rows, cols = out.shape
    total = arrived[0].astype(jnp.float32)
    for chip in range(1, arrived.shape[0]):
        total += arrived[chip].astype(jnp.float32)
    total = total.astype(out.dtype)
    out[:, :LANES] = total[:rows]
    tail = total[rows:]
    out[: rows // 2, LANES:] = tail[:, : cols - LANES]
    out[rows // 2 :, LANES:] = tail[:, cols - LANES :]


def local(tokens, norm_gain, up_trained, down_trained):
    chips, cores, groups = lax.axis_size("z"), lax.axis_size("core"), lax.axis_size("tp")
    shards = chips * cores
    rows_local, cols_local = up_trained.shape
    count, features = tokens.shape
    width = cols_local * groups // shards
    blocks = cols_local // (width * cores)
    quarter = rows_local // groups
    where = jnp.stack([lax.axis_index("tp"), lax.axis_index("core"), lax.axis_index("member")]).astype(jnp.int32)
    smem, vmem = pl.BlockSpec(memory_space=pltpu.SMEM), pl.BlockSpec(memory_space=pltpu.VMEM)
    first = lax.axis_index("member") == 0
    mine = jnp.where(first, norm_gain[:, None] * up_trained, down_trained).astype(jnp.bfloat16)
    pieces = mine.reshape(groups, quarter, blocks, cores, width).transpose(3, 0, 2, 1, 4)
    pieces = pieces.reshape(cores * groups, blocks, quarter, width)
    moved = lax.all_to_all(pieces, ("core", "tp"), 0, 0, tiled=True)
    moved = moved.reshape(cores, chips, quarter, width).transpose(1, 0, 2, 3)
    own = lax.all_to_all(moved, "z", 0, 0, tiled=True).reshape(shards, quarter, width)
    half = shards // 2
    values = tokens.astype(jnp.float32)
    scale = lax.rsqrt(jnp.mean(values * values, axis=1, keepdims=True) + epsilon)
    normed = (values * scale).astype(jnp.bfloat16)

    twin = lax.ppermute(own, "member", ring(PAIR, 1))
    right = lax.ppermute(own, "tp", ring(groups, 1))
    left = lax.ppermute(own, "tp", ring(groups, -1))
    twin_right = lax.ppermute(twin, "tp", ring(groups, 1))
    twin_left = lax.ppermute(twin, "tp", ring(groups, -1))
    far_first = lax.ppermute(right[:half], "tp", ring(groups, 1))
    far_second = lax.ppermute(left[half:], "tp", ring(groups, -1))
    twin_far_second = lax.ppermute(right[half:], ("member", "tp"), across(groups, 1))
    twin_far_first = lax.ppermute(left[:half], ("member", "tp"), across(groups, -1))
    served = jax.ShapeDtypeStruct((shards, groups, quarter, width), jnp.bfloat16)
    part = jax.ShapeDtypeStruct((chips, rows_local * count // LANES, LANES), jnp.bfloat16)
    up, down, active, away = pl.pallas_call(
        functools.partial(feed_forward, cores),
        out_shape=[served, served, jax.ShapeDtypeStruct((count, width), jnp.bfloat16), part],
        in_specs=[smem] + [vmem] * 11,
        out_specs=[vmem] * 4,
        compiler_params=pltpu.CompilerParams(vmem_limit_bytes=24 << 20),
        cost_estimate=pl.CostEstimate(
            flops=3 * count * features * width, bytes_accessed=8 * features * width, transcendentals=0
        ),
        name="feed_forward",
    )(
        where, normed, own, left, far_first, far_second, right,
        twin, twin_left, twin_far_first, twin_far_second, twin_right,
    )
    up_serving, down_serving, kept = pl.pallas_call(
        functools.partial(own_side, cores),
        out_shape=[served, served, part],
        in_specs=[smem] + [vmem] * 3,
        out_specs=[pl.BlockSpec(memory_space=pl.ANY)] * 2 + [vmem],
        scratch_shapes=[pltpu.SemaphoreType.DMA((2,))],
        compiler_params=pltpu.CompilerParams(vmem_limit_bytes=16 << 20),
        cost_estimate=pl.CostEstimate(
            flops=count * features * width, bytes_accessed=8 * features * width, transcendentals=0
        ),
        name="own_side",
    )(where, active, up, down)
    swapped = lax.ppermute(away, "core", ring(cores, 1))
    arrived = lax.all_to_all(added(kept, swapped), "z", 0, 0, tiled=True)
    out = pl.pallas_call(
        summed_up,
        out_shape=jax.ShapeDtypeStruct((rows_local, count), jnp.bfloat16),
        in_specs=[vmem],
        out_specs=vmem,
        compiler_params=pltpu.CompilerParams(vmem_limit_bytes=8 << 20),
        name="summed_up",
    )(arrived).T
    return (up_serving.reshape(features, width), down_serving.reshape(features, width), out)


def solution(mesh):
    sizes = mesh.shape
    devices = mesh.devices.reshape(sizes["grp"] // PAIR, PAIR, sizes["fs"] // CORES, CORES, sizes["tp"])
    split = jax.sharding.Mesh(devices, ("pair", "member", "z", "core", "tp"))
    grp, fs = ("pair", "member"), ("z", "core")
    in_specs = (P((*grp, "tp"), None), P(fs), P(fs, "tp"), P(fs, "tp"))
    out_specs = (P(grp, fs), P(grp, fs), P((*grp, "tp"), fs))

    return jax.shard_map(local, mesh=split, in_specs=in_specs, out_specs=out_specs, check_vma=False)
```

profile of v0, /device:TPU:40, one launch (start us, length us, event | category | flops | bytes accessed | tf_op | source)
XLA Modules:
  0.0 116.0 jit_solution(1023155816975898005)
XLA Ops:
  0.6 1.3 %select_convert_fusion = bf16[64,2048]{1,0:T(8,128)(2,1)S(1)} fusion(f32[64,2048]{1,0:T(8,128)} %param.7, f32[64,2048]{1,0:T(8,128)} %param.6, f32[64]{0:T(128)} %param.5, pred[]{:T(512)S(6)} %eq.3), kind=kLoop, calls=%fused_computation.5 | loop fusion | flops 262144 | bytes 1310977 | tf_op jit(solution)/shard_map/convert_element_type | solution.py:115
  2.0 0.2 reshape.33
  2.1 0.0 copy-start
  2.2 11.4 %all_to_all.15 = bf16[8,4,16,256]{3,2,1,0:T(8,128)(2,1)S(1)} all-to-all(bf16[8,4,16,256]{3,2,1,0:T(8,128)(2,1)S(1)} %bitcast.17), channel_id=1, replica_groups=mesh['pair'=1,'member'=2,'z'=16,'core'=2,'tp'=4] {'core','tp'}, dimensions={0} | all-to-all | bytes 524288 | tf_op jit(solution)/shard_map/all_to_all | solution.py:118
  13.6 42.1 %all_to_all.16 = bf16[16,2,16,256]{3,2,1,0:T(8,128)(2,1)S(1)} all-to-all(bf16[16,2,16,256]{3,2,1,0:T(8,128)(2,1)S(1)} %copy.11), channel_id=1, replica_groups=mesh['pair'=1,'member'=2,'z'=16,'core'=2,'tp'=4] {'z'}, dimensions={0} | all-to-all | bytes 524288 | tf_op jit(solution)/shard_map/all_to_all | solution.py:120
  55.7 0.9 collective-permute-start.1
  56.6 0.2 fusion
  56.8 2.5 %collective-permute-start = (bf16[32,16,256]{2,1,0:T(8,128)(2,1)S(1)}, bf16[32,16,256]{2,1,0:T(8,128)(2,1)S(1)}, u32[]{:S(2)}, u32[]{:S(2)}) collective-permute-start(bf16[32,16,256]{2,1,0:T(8,128)(2,1)S(1)} %bitcast.13), channel_id=1, source_target_pairs={{0,3},{1,0},{2,1},{3,2},{4,7},{5,4},{6,5},{7,6},{8,11},{9,8},{10,9... | collective-permute-start | bytes 786440 | tf_op jit(solution)/shard_map/ppermute | solution.py:128
  59.3 6.8 %collective-permute-done.1.refs_4_ = bf16[32,16,256]{2,1,0:T(8,128)(2,1)S(1)} collective-permute-done((bf16[32,16,256]{2,1,0:T(8,128)(2,1)S(1)}, bf16[32,16,256]{2,1,0:T(8,128)(2,1)S(1)}, u32[]{:S(2)}, u32[]{:S(2)}) %collective-permute-start.1) | collective-permute-done | bytes 262176 | tf_op jit(solution)/shard_map/ppermute | solution.py:127
  66.1 0.1 collective-permute-start.7
  66.3 0.1 collective-permute-start.2
  66.5 4.1 %collective-permute-start.6 = (bf16[16,16,256]{2,1,0:T(8,128)(2,1)S(1)}, bf16[16,16,256]{2,1,0:T(8,128)(2,1)S(1)}, u32[]{:S(2)}, u32[]{:S(2)}) collective-permute-start(bf16[16,16,256]{2,1,0:T(8,128)(2,1)S(1)} %get-tuple-element.19), channel_id=1, source_target_pairs={{0,131},{1,128},{2,129},{3,130},{128,3},{129,0},{130,1},{131,2},{4... | collective-permute-start | bytes 393224 | tf_op jit(solution)/shard_map/ppermute | solution.py:134
  70.5 2.0 %collective-permute-start.3 = (bf16[16,16,256]{2,1,0:T(8,128)(2,1)S(1)}, bf16[16,16,256]{2,1,0:T(8,128)(2,1)S(1)}, u32[]{:S(2)}, u32[]{:S(2)}) collective-permute-start(bf16[16,16,256]{2,1,0:T(8,128)(2,1)S(1)} %get-tuple-element.20), channel_id=1, source_target_pairs={{0,3},{1,0},{2,1},{3,2},{4,7},{5,4},{6,5},{7,6},{8,11},{9,8},{10,9... | collective-permute-start | bytes 393224 | tf_op jit(solution)/shard_map/ppermute | solution.py:132
  72.6 0.9 collective-permute-done.7.refs_8_
  73.4 2.4 %collective-permute-start.5 = (bf16[32,16,256]{2,1,0:T(8,128)(2,1)S(1)}, bf16[32,16,256]{2,1,0:T(8,128)(2,1)S(1)}, u32[]{:S(2)}, u32[]{:S(2)}) collective-permute-start(bf16[32,16,256]{2,1,0:T(8,128)(2,1)S(1)} %collective-permute-done.4.refs_5_), channel_id=1, source_target_pairs={{0,3},{1,0},{2,1},{3,2},{4,7},{5,4},{6,5},{7,6},{8,11},{9,8},{10,9... | collective-permute-start | bytes 786440 | tf_op jit(solution)/shard_map/ppermute | solution.py:130
  75.8 0.2 fusion.1.normed
  76.0 0.1 pad_add_fusion.where
  76.1 4.0 %collective-permute-done.8.refs_9_ = bf16[32,16,256]{2,1,0:T(8,128)(2,1)S(1)} collective-permute-done((bf16[32,16,256]{2,1,0:T(8,128)(2,1)S(1)}, bf16[32,16,256]{2,1,0:T(8,128)(2,1)S(1)}, u32[]{:S(2)}, u32[]{:S(2)}) %collective-permute-start.8) | collective-permute-done | bytes 262176 | tf_op jit(solution)/shard_map/ppermute | solution.py:129
  80.1 1.8 %feed_forward.1 = (bf16[32,4,16,256]{3,2,1,0:T(8,128)(2,1)S(1)}, bf16[32,4,16,256]{3,2,1,0:T(8,128)(2,1)S(1)}, bf16[192,256]{1,0:T(8,128)(2,1)S(1)}, bf16[16,96,128]{2,1,0:T(8,128)(2,1)S(1)}) custom-call(s32[3]{0:T(128)S(1)} %pad_add_fusion.where, bf16[192,2048]{1,0:T(8,128)(2,1)S(1)} %fusion.1.normed, bf16[32,16,256]{2,1,0:T(8,128)(2,1)S(1)} %bitcast.15, ...), custom_call_target="tpu_custom_call" | custom-call | flops 301989888 | bytes 4194304 | tf_op jit(solution)/shard_map/feed_forward/pallas_call | solution.py:137
  82.0 0.1 collective-permute-start.9
  82.1 1.9 %own_side.1 = (bf16[32,4,16,256]{3,2,1,0:T(8,128)(2,1)}, bf16[32,4,16,256]{3,2,1,0:T(8,128)(2,1)}, bf16[16,96,128]{2,1,0:T(8,128)(2,1)S(1)}) custom-call(s32[3]{0:T(128)S(1)} %pad_add_fusion.where, bf16[192,256]{1,0:T(8,128)(2,1)S(1)} %get-tuple-element.10.active, bf16[32,4,16,256]{3,2,1,0:T(8,128)(2,1)S(1)} %get-tuple-element.11.up, ...), custom_call_target="tpu_custom_call" | custom-call | flops 100663296 | bytes 4194304 | tf_op jit(solution)/shard_map/own_side/pallas_call | solution.py:151
  84.0 0.1 add_convert_fusion
  84.2 31.2 %all_to_all.17.arrived = bf16[16,96,128]{2,1,0:T(8,128)(2,1)S(1)} all-to-all(bf16[16,96,128]{2,1,0:T(8,128)(2,1)S(1)} %add_convert_fusion), channel_id=1, replica_groups=mesh['pair'=1,'member'=2,'z'=16,'core'=2,'tp'=4] {'z'}, dimensions={0} | all-to-all | bytes 786432 | tf_op jit(solution)/shard_map/all_to_all | solution.py:164
  115.3 0.7 summed_up.1
  (15 shorter events, 0.1 us)
Async XLA Ops:
  2.1 54.4 %copy-start = (bf16[192,2048]{1,0:T(8,128)(2,1)S(1)}, bf16[192,2048]{1,0:T(8,128)(2,1)}, u32[]{:S(2)}) copy-start(bf16[192,2048]{1,0:T(8,128)(2,1)} %param.4) | copy-start | bytes 2359300
  55.7 10.4 %collective-permute-start.1 = (bf16[32,16,256]{2,1,0:T(8,128)(2,1)S(1)}, bf16[32,16,256]{2,1,0:T(8,128)(2,1)S(1)}, u32[]{:S(2)}, u32[]{:S(2)}) collective-permute-start(bf16[32,16,256]{2,1,0:T(8,128)(2,1)S(1)} %bitcast.12), channel_id=1, source_target_pairs={{0,1},{1,2},{2,3},{3,0},{4,5},{5,6},{6,7},{7,4},{8,9},{9,10},{10,1... | collective-permute-start | bytes 786440 | tf_op jit(solution)/shard_map/ppermute | solution.py:127
  56.8 9.6 %collective-permute-start = (bf16[32,16,256]{2,1,0:T(8,128)(2,1)S(1)}, bf16[32,16,256]{2,1,0:T(8,128)(2,1)S(1)}, u32[]{:S(2)}, u32[]{:S(2)}) collective-permute-start(bf16[32,16,256]{2,1,0:T(8,128)(2,1)S(1)} %bitcast.13), channel_id=1, source_target_pairs={{0,3},{1,0},{2,1},{3,2},{4,7},{5,4},{6,5},{7,6},{8,11},{9,8},{10,9... | collective-permute-start | bytes 786440 | tf_op jit(solution)/shard_map/ppermute | solution.py:128
  59.3 13.2 %collective-permute-start.4 = (bf16[32,16,256]{2,1,0:T(8,128)(2,1)S(1)}, bf16[32,16,256]{2,1,0:T(8,128)(2,1)S(1)}, u32[]{:S(2)}, u32[]{:S(2)}) collective-permute-start(bf16[32,16,256]{2,1,0:T(8,128)(2,1)S(1)} %bitcast.14), channel_id=1, source_target_pairs={{0,128},{128,0},{1,129},{129,1},{2,130},{130,2},{3,131},{131,3},{4... | collective-permute-start | bytes 786440 | tf_op jit(solution)/shard_map/ppermute | solution.py:126
  66.1 7.3 %collective-permute-start.7 = (bf16[16,16,256]{2,1,0:T(8,128)(2,1)S(1)}, bf16[16,16,256]{2,1,0:T(8,128)(2,1)S(1)}, u32[]{:S(2)}, u32[]{:S(2)}) collective-permute-start(bf16[16,16,256]{2,1,0:T(8,128)(2,1)S(1)} %get-tuple-element.17), channel_id=1, source_target_pairs={{0,129},{1,130},{2,131},{3,128},{128,1},{129,2},{130,3},{131,0},{4... | collective-permute-start | bytes 393224 | tf_op jit(solution)/shard_map/ppermute | solution.py:133
  66.3 9.8 %collective-permute-start.2 = (bf16[16,16,256]{2,1,0:T(8,128)(2,1)S(1)}, bf16[16,16,256]{2,1,0:T(8,128)(2,1)S(1)}, u32[]{:S(2)}, u32[]{:S(2)}) collective-permute-start(bf16[16,16,256]{2,1,0:T(8,128)(2,1)S(1)} %get-tuple-element.18), channel_id=1, source_target_pairs={{0,1},{1,2},{2,3},{3,0},{4,5},{5,6},{6,7},{7,4},{8,9},{9,10},{10,1... | collective-permute-start | bytes 393224 | tf_op jit(solution)/shard_map/ppermute | solution.py:131
  66.5 9.6 %collective-permute-start.6 = (bf16[16,16,256]{2,1,0:T(8,128)(2,1)S(1)}, bf16[16,16,256]{2,1,0:T(8,128)(2,1)S(1)}, u32[]{:S(2)}, u32[]{:S(2)}) collective-permute-start(bf16[16,16,256]{2,1,0:T(8,128)(2,1)S(1)} %get-tuple-element.19), channel_id=1, source_target_pairs={{0,131},{1,128},{2,129},{3,130},{128,3},{129,0},{130,1},{131,2},{4... | collective-permute-start | bytes 393224 | tf_op jit(solution)/shard_map/ppermute | solution.py:134
  70.5 5.6 %collective-permute-start.3 = (bf16[16,16,256]{2,1,0:T(8,128)(2,1)S(1)}, bf16[16,16,256]{2,1,0:T(8,128)(2,1)S(1)}, u32[]{:S(2)}, u32[]{:S(2)}) collective-permute-start(bf16[16,16,256]{2,1,0:T(8,128)(2,1)S(1)} %get-tuple-element.20), channel_id=1, source_target_pairs={{0,3},{1,0},{2,1},{3,2},{4,7},{5,4},{6,5},{7,6},{8,11},{9,8},{10,9... | collective-permute-start | bytes 393224 | tf_op jit(solution)/shard_map/ppermute | solution.py:132
  72.6 7.6 %collective-permute-start.8 = (bf16[32,16,256]{2,1,0:T(8,128)(2,1)S(1)}, bf16[32,16,256]{2,1,0:T(8,128)(2,1)S(1)}, u32[]{:S(2)}, u32[]{:S(2)}) collective-permute-start(bf16[32,16,256]{2,1,0:T(8,128)(2,1)S(1)} %collective-permute-done.4.refs_5_), channel_id=1, source_target_pairs={{0,1},{1,2},{2,3},{3,0},{4,5},{5,6},{6,7},{7,4},{8,9},{9,10},{10,1... | collective-permute-start | bytes 786440 | tf_op jit(solution)/shard_map/ppermute | solution.py:129
  73.4 6.7 %collective-permute-start.5 = (bf16[32,16,256]{2,1,0:T(8,128)(2,1)S(1)}, bf16[32,16,256]{2,1,0:T(8,128)(2,1)S(1)}, u32[]{:S(2)}, u32[]{:S(2)}) collective-permute-start(bf16[32,16,256]{2,1,0:T(8,128)(2,1)S(1)} %collective-permute-done.4.refs_5_), channel_id=1, source_target_pairs={{0,3},{1,0},{2,1},{3,2},{4,7},{5,4},{6,5},{7,6},{8,11},{9,8},{10,9... | collective-permute-start | bytes 786440 | tf_op jit(solution)/shard_map/ppermute | solution.py:130
  82.0 2.0 %collective-permute-start.9 = (bf16[16,96,128]{2,1,0:T(8,128)(2,1)S(1)}, bf16[16,96,128]{2,1,0:T(8,128)(2,1)S(1)}, u32[]{:S(2)}, u32[]{:S(2)}) collective-permute-start(bf16[16,96,128]{2,1,0:T(8,128)(2,1)S(1)} %get-tuple-element.16), channel_id=1, source_target_pairs={{0,4},{4,0},{1,5},{5,1},{2,6},{6,2},{3,7},{7,3},{8,12},{12,8},{9,1... | collective-permute-start | bytes 1179656 | tf_op jit(solution)/shard_map/ppermute | solution.py:163
where the time goes:
time: 117 us; the launch traced here: 116 us
  blocking collectives  84.6 us (72%)
  starting transfers between devices  12.2 us (10%)
  waiting for transfers between devices  11.7 us (10%)
  Pallas kernels  4.43 us (4%)
  other arithmetic  1.94 us (2%)
    all_to_all x1, blocking collectives, local(): lax.all_to_all(moved, 'z', 0, 0, tiled=True).reshape(shards, quarter, width)  42.1 us
    all_to_all x1, blocking collectives, local(): arrived = lax.all_to_all(added(kept, swapped), 'z', 0, 0, tiled=True)  31.2 us
    all_to_all x1, blocking collectives, local(): moved = lax.all_to_all(pieces, ('core', 'tp'), 0, 0, tiled=True)  11.4 us
    ppermute x1, waiting for transfers between devices, local(): right = lax.ppermute(own, 'tp', ring(groups, 1))  6.8 us
    ppermute x1, starting transfers between devices, local(): lax.ppermute(left[:half], ('member', 'tp'), across(groups, -1))  4.07 us
    ppermute x1, waiting for transfers between devices, local(): twin_right = lax.ppermute(twin, 'tp', ring(groups, 1))  4.05 us
    ppermute x1, starting transfers between devices, local(): left = lax.ppermute(own, 'tp', ring(groups, -1))  2.48 us
    ppermute x1, starting transfers between devices, local(): twin_left = lax.ppermute(twin, 'tp', ring(groups, -1))  2.37 us
  transfers between devices with their start and end apart: 10, of which 3 were waited for; matrix products, arithmetic and copies ran while one was open for 0% of the time, Pallas kernels for 2%

commit v1 on v0

--- a/solution.py
+++ b/solution.py
@@ -49,24 +49,21 @@
     shards, groups, quarter, width = up.shape
     at, core, member = where[0], where[1], where[2]
 
-    def place(weight, own, left, far_first, far_second, right):
-        half = shards // 2
-        for step, first, count, piece in (
-            (0, 0, shards, own),
-            (1, 0, shards, left),
-            (2, 0, half, far_first),
-            (2, half, half, far_second),
-            (3, 0, shards, right),
-        ):
-            slot = lax.rem(at + step, groups)
-            weight[pl.ds(first, count), pl.ds(slot, 1)] = piece[...][:, None]
+    def place(weight, *pieces):
+        for step, parts in enumerate(pieces):
+            slot, first = lax.rem(at + step, groups), 0
+            for part in parts:
+                count = part.shape[0]
+                weight[pl.ds(first, count), pl.ds(slot, 1)] = part[...][:, None]
+                first += count
 
+    own, left, far, right, twin, *rest, twin_right = quarters
     for value, mine, other in ((0, up, down), (1, down, up)):
 
         @pl.when(member == value)
         def _(mine=mine, other=other):
-            place(mine, *quarters[:5])
-            place(other, *quarters[5:])
+            place(mine, [own], [left], [far], [right])
+            place(other, [twin], rest[:2], rest[2:], [twin_right])
 
     hidden = jnp.dot(
         normed[...], up[...].reshape(shards * groups * quarter, width), preferred_element_type=jnp.float32
@@ -118,20 +115,20 @@
     moved = lax.all_to_all(pieces, ("core", "tp"), 0, 0, tiled=True)
     moved = moved.reshape(cores, chips, quarter, width).transpose(1, 0, 2, 3)
     own = lax.all_to_all(moved, "z", 0, 0, tiled=True).reshape(shards, quarter, width)
-    half = shards // 2
     values = tokens.astype(jnp.float32)
     scale = lax.rsqrt(jnp.mean(values * values, axis=1, keepdims=True) + epsilon)
     normed = (values * scale).astype(jnp.bfloat16)
 
     twin = lax.ppermute(own, "member", ring(PAIR, 1))
+    left = lax.ppermute(own, "tp", ring(groups, -1))
     right = lax.ppermute(own, "tp", ring(groups, 1))
-    left = lax.ppermute(own, "tp", ring(groups, -1))
+    cut, far_cut = shards * 5 // 8, shards * 3 // 8
     twin_right = lax.ppermute(twin, "tp", ring(groups, 1))
-    twin_left = lax.ppermute(twin, "tp", ring(groups, -1))
-    far_first = lax.ppermute(right[:half], "tp", ring(groups, 1))
-    far_second = lax.ppermute(left[half:], "tp", ring(groups, -1))
-    twin_far_second = lax.ppermute(right[half:], ("member", "tp"), across(groups, 1))
-    twin_far_first = lax.ppermute(left[:half], ("member", "tp"), across(groups, -1))
+    far = lax.ppermute(left, "tp", ring(groups, -1))
+    twin_left_first = lax.ppermute(left[:cut], "member", ring(PAIR, 1))
+    twin_far_second = lax.ppermute(right[far_cut:], ("member", "tp"), across(groups, 1))
+    twin_left_second = lax.ppermute(twin[cut:], "tp", ring(groups, -1))
+    twin_far_first = lax.ppermute(left[:far_cut], ("member", "tp"), across(groups, -1))
     served = jax.ShapeDtypeStruct((shards, groups, quarter, width), jnp.bfloat16)
     part = jax.ShapeDtypeStruct((chips, rows_local * count // LANES, LANES), jnp.bfloat16)
     up, down, active, away = pl.pallas_call(
@@ -145,8 +142,8 @@
         ),
         name="feed_forward",
     )(
-        where, normed, own, left, far_first, far_second, right,
-        twin, twin_left, twin_far_first, twin_far_second, twin_right,
+        where, normed, own, left, far, right,
+        twin, twin_left_first, twin_left_second, twin_far_first, twin_far_second, twin_right,
     )
     up_serving, down_serving, kept = pl.pallas_call(
         functools.partial(own_side, cores),

time: 117 us -> 115 us (0.983)
  waiting for transfers between devices: 11.7 us -> 8.58 us
    ppermute x1, waiting for transfers between devices: 6.8 us -> 1.28 us  [local(): right = lax.ppermute(own, 'tp', ring(groups, 1))]
    ppermute x1, waiting for transfers between devices: 0.01 us -> 4.58 us  [local(): twin = lax.ppermute(own, 'member', ring(PAIR, 1))]
    ppermute x1, waiting for transfers between devices: 4.05 us -> 0.01 us  [local(): twin_right = lax.ppermute(twin, 'tp', ring(groups, 1))]
    ppermute x5, waiting for transfers between devices: 0.88 us -> 2.71 us  [the longest x1 2.69 us: local(): lax.ppermute(left[:far_cut], ('member', 'tp'), across(groups, -1))]
where the time goes in v1:
time: 115 us; the launch traced here: 114 us
  blocking collectives  84.9 us (74%)
  starting transfers between devices  13 us (11%)
  waiting for transfers between devices  8.58 us (7%)
  Pallas kernels  4.44 us (4%)
  other arithmetic  1.94 us (2%)
    all_to_all x1, blocking collectives, local(): lax.all_to_all(moved, 'z', 0, 0, tiled=True).reshape(shards, quarter, width)  42.1 us
    all_to_all x1, blocking collectives, local(): arrived = lax.all_to_all(added(kept, swapped), 'z', 0, 0, tiled=True)  31.4 us
    all_to_all x1, blocking collectives, local(): moved = lax.all_to_all(pieces, ('core', 'tp'), 0, 0, tiled=True)  11.4 us
    ppermute x1, waiting for transfers between devices, local(): twin = lax.ppermute(own, 'member', ring(PAIR, 1))  4.58 us
    ppermute x1, starting transfers between devices, local(): lax.ppermute(left[:far_cut], ('member', 'tp'), across(groups, -1))  2.86 us
    ppermute x1, starting transfers between devices, local(): far = lax.ppermute(left, 'tp', ring(groups, -1))  2.77 us
    ppermute x1, starting transfers between devices, local(): lax.ppermute(right[far_cut:], ('member', 'tp'), across(groups, 1))  2.76 us
    ppermute x1, waiting for transfers between devices, local(): lax.ppermute(left[:far_cut], ('member', 'tp'), across(groups, -1))  2.69 us
  transfers between devices with their start and end apart: 10, of which 3 were waited for; matrix products, arithmetic and copies ran while one was open for 0% of the time, Pallas kernels for 2%

profile of v1, /device:TPU:40, one launch (start us, length us, event | category | flops | bytes accessed | tf_op | source)
XLA Modules:
  0.0 113.9 jit_solution(1342835790162080866)
XLA Ops:
  0.6 1.3 %select_convert_fusion = bf16[64,2048]{1,0:T(8,128)(2,1)S(1)} fusion(f32[64,2048]{1,0:T(8,128)} %param.7, f32[64,2048]{1,0:T(8,128)} %param.6, f32[64]{0:T(128)} %param.5, pred[]{:T(512)S(6)} %eq.3), kind=kLoop, calls=%fused_computation.5 | loop fusion | flops 262144 | bytes 1310977 | tf_op jit(solution)/shard_map/convert_element_type | solution.py:112
  2.0 0.2 reshape.33
  2.2 11.4 %all_to_all.15 = bf16[8,4,16,256]{3,2,1,0:T(8,128)(2,1)S(1)} all-to-all(bf16[8,4,16,256]{3,2,1,0:T(8,128)(2,1)S(1)} %bitcast.17), channel_id=1, replica_groups=mesh['pair'=1,'member'=2,'z'=16,'core'=2,'tp'=4] {'core','tp'}, dimensions={0} | all-to-all | bytes 524288 | tf_op jit(solution)/shard_map/all_to_all | solution.py:115
  13.6 42.1 %all_to_all.16 = bf16[16,2,16,256]{3,2,1,0:T(8,128)(2,1)S(1)} all-to-all(bf16[16,2,16,256]{3,2,1,0:T(8,128)(2,1)S(1)} %copy.11), channel_id=1, replica_groups=mesh['pair'=1,'member'=2,'z'=16,'core'=2,'tp'=4] {'z'}, dimensions={0} | all-to-all | bytes 524288 | tf_op jit(solution)/shard_map/all_to_all | solution.py:117
  55.7 0.9 collective-permute-start.2
  56.6 2.4 %collective-permute-start = (bf16[32,16,256]{2,1,0:T(8,128)(2,1)S(1)}, bf16[32,16,256]{2,1,0:T(8,128)(2,1)S(1)}, u32[]{:S(2)}, u32[]{:S(2)}) collective-permute-start(bf16[32,16,256]{2,1,0:T(8,128)(2,1)S(1)} %bitcast.14), channel_id=1, source_target_pairs={{0,3},{1,0},{2,1},{3,2},{4,7},{5,4},{6,5},{7,6},{8,11},{9,8},{10,9... | collective-permute-start | bytes 786440 | tf_op jit(solution)/shard_map/ppermute | solution.py:123
  59.0 0.2 fusion
  59.2 4.6 %collective-permute-done.3.refs_4_ = bf16[32,16,256]{2,1,0:T(8,128)(2,1)S(1)} collective-permute-done((bf16[32,16,256]{2,1,0:T(8,128)(2,1)S(1)}, bf16[32,16,256]{2,1,0:T(8,128)(2,1)S(1)}, u32[]{:S(2)}, u32[]{:S(2)}) %collective-permute-start.3) | collective-permute-done | bytes 262176 | tf_op jit(solution)/shard_map/ppermute | solution.py:122
  63.8 0.5 collective-permute-start.5
  64.3 1.3 %collective-permute-done.2.refs_3_ = bf16[32,16,256]{2,1,0:T(8,128)(2,1)S(1)} collective-permute-done((bf16[32,16,256]{2,1,0:T(8,128)(2,1)S(1)}, bf16[32,16,256]{2,1,0:T(8,128)(2,1)S(1)}, u32[]{:S(2)}, u32[]{:S(2)}) %collective-permute-start.2) | collective-permute-done | bytes 262176 | tf_op jit(solution)/shard_map/ppermute | solution.py:124
  65.6 2.8 %collective-permute-start.7 = (bf16[20,16,256]{2,1,0:T(8,128)(2,1)S(1)}, bf16[20,16,256]{2,1,0:T(8,128)(2,1)S(1)}, u32[]{:S(2)}, u32[]{:S(2)}) collective-permute-start(bf16[20,16,256]{2,1,0:T(8,128)(2,1)S(1)} %slice.19), channel_id=1, source_target_pairs={{0,129},{1,130},{2,131},{3,128},{128,1},{129,2},{130,3},{131,0},{4... | collective-permute-start | bytes 491528 | tf_op jit(solution)/shard_map/ppermute | solution.py:129
  68.4 0.1 collective-permute-start.4
  68.5 0.6 collective-permute-start.8
  69.1 2.8 %collective-permute-start.1 = (bf16[32,16,256]{2,1,0:T(8,128)(2,1)S(1)}, bf16[32,16,256]{2,1,0:T(8,128)(2,1)S(1)}, u32[]{:S(2)}, u32[]{:S(2)}) collective-permute-start(bf16[32,16,256]{2,1,0:T(8,128)(2,1)S(1)} %collective-permute-done.refs_1_), channel_id=1, source_target_pairs={{0,3},{1,0},{2,1},{3,2},{4,7},{5,4},{6,5},{7,6},{8,11},{9,8},{10,9... | collective-permute-start | bytes 786440 | tf_op jit(solution)/shard_map/ppermute | solution.py:127
  71.9 0.2 fusion.1.normed
  72.1 2.9 %collective-permute-start.6 = (bf16[12,16,256]{2,1,0:T(8,128)(2,1)S(1)}, bf16[12,16,256]{2,1,0:T(8,128)(2,1)S(1)}, u32[]{:S(2)}, u32[]{:S(2)}) collective-permute-start(bf16[12,16,256]{2,1,0:T(8,128)(2,1)S(1)} %slice.18), channel_id=1, source_target_pairs={{0,131},{1,128},{2,129},{3,130},{128,3},{129,0},{130,1},{131,2},{4... | collective-permute-start | bytes 294920 | tf_op jit(solution)/shard_map/ppermute | solution.py:131
  75.0 0.1 pad_add_fusion.where
  75.0 2.7 %collective-permute-done.6.refs_7_ = bf16[12,16,256]{2,1,0:T(8,128)(2,1)S(1)} collective-permute-done((bf16[12,16,256]{2,1,0:T(8,128)(2,1)S(1)}, bf16[12,16,256]{2,1,0:T(8,128)(2,1)S(1)}, u32[]{:S(2)}, u32[]{:S(2)}) %collective-permute-start.6) | collective-permute-done | bytes 98336 | tf_op jit(solution)/shard_map/ppermute | solution.py:131
  77.7 1.8 %feed_forward.1 = (bf16[32,4,16,256]{3,2,1,0:T(8,128)(2,1)S(1)}, bf16[32,4,16,256]{3,2,1,0:T(8,128)(2,1)S(1)}, bf16[192,256]{1,0:T(8,128)(2,1)S(1)}, bf16[16,96,128]{2,1,0:T(8,128)(2,1)S(1)}) custom-call(s32[3]{0:T(128)S(1)} %pad_add_fusion.where, bf16[192,2048]{1,0:T(8,128)(2,1)S(1)} %fusion.1.normed, bf16[32,16,256]{2,1,0:T(8,128)(2,1)S(1)} %bitcast.15, ...), custom_call_target="tpu_custom_call" | custom-call | flops 301989888 | bytes 4194304 | tf_op jit(solution)/shard_map/feed_forward/pallas_call | solution.py:134
  79.6 0.1 collective-permute-start.9
  79.7 1.9 %own_side.1 = (bf16[32,4,16,256]{3,2,1,0:T(8,128)(2,1)}, bf16[32,4,16,256]{3,2,1,0:T(8,128)(2,1)}, bf16[16,96,128]{2,1,0:T(8,128)(2,1)S(1)}) custom-call(s32[3]{0:T(128)S(1)} %pad_add_fusion.where, bf16[192,256]{1,0:T(8,128)(2,1)S(1)} %get-tuple-element.10.active, bf16[32,4,16,256]{3,2,1,0:T(8,128)(2,1)S(1)} %get-tuple-element.11.up, ...), custom_call_target="tpu_custom_call" | custom-call | flops 100663296 | bytes 4194304 | tf_op jit(solution)/shard_map/own_side/pallas_call | solution.py:148
  81.6 0.1 add_convert_fusion
  81.8 31.4 %all_to_all.17.arrived = bf16[16,96,128]{2,1,0:T(8,128)(2,1)S(1)} all-to-all(bf16[16,96,128]{2,1,0:T(8,128)(2,1)S(1)} %add_convert_fusion), channel_id=1, replica_groups=mesh['pair'=1,'member'=2,'z'=16,'core'=2,'tp'=4] {'z'}, dimensions={0} | all-to-all | bytes 786432 | tf_op jit(solution)/shard_map/all_to_all | solution.py:161
  113.2 0.7 summed_up.1
  (17 shorter events, 0.1 us)
Async XLA Ops:
  2.1 56.8 %copy-start = (bf16[192,2048]{1,0:T(8,128)(2,1)S(1)}, bf16[192,2048]{1,0:T(8,128)(2,1)}, u32[]{:S(2)}) copy-start(bf16[192,2048]{1,0:T(8,128)(2,1)} %param.4) | copy-start | bytes 2359300
  55.7 8.1 %collective-permute-start.3 = (bf16[32,16,256]{2,1,0:T(8,128)(2,1)S(1)}, bf16[32,16,256]{2,1,0:T(8,128)(2,1)S(1)}, u32[]{:S(2)}, u32[]{:S(2)}) collective-permute-start(bf16[32,16,256]{2,1,0:T(8,128)(2,1)S(1)} %bitcast.12), channel_id=1, source_target_pairs={{0,128},{128,0},{1,129},{129,1},{2,130},{130,2},{3,131},{131,3},{4... | collective-permute-start | bytes 786440 | tf_op jit(solution)/shard_map/ppermute | solution.py:122
  55.7 9.8 %collective-permute-start.2 = (bf16[32,16,256]{2,1,0:T(8,128)(2,1)S(1)}, bf16[32,16,256]{2,1,0:T(8,128)(2,1)S(1)}, u32[]{:S(2)}, u32[]{:S(2)}) collective-permute-start(bf16[32,16,256]{2,1,0:T(8,128)(2,1)S(1)} %bitcast.13), channel_id=1, source_target_pairs={{0,1},{1,2},{2,3},{3,0},{4,5},{5,6},{6,7},{7,4},{8,9},{9,10},{10,1... | collective-permute-start | bytes 786440 | tf_op jit(solution)/shard_map/ppermute | solution.py:124
  56.6 11.8 %collective-permute-start = (bf16[32,16,256]{2,1,0:T(8,128)(2,1)S(1)}, bf16[32,16,256]{2,1,0:T(8,128)(2,1)S(1)}, u32[]{:S(2)}, u32[]{:S(2)}) collective-permute-start(bf16[32,16,256]{2,1,0:T(8,128)(2,1)S(1)} %bitcast.14), channel_id=1, source_target_pairs={{0,3},{1,0},{2,1},{3,2},{4,7},{5,4},{6,5},{7,6},{8,11},{9,8},{10,9... | collective-permute-start | bytes 786440 | tf_op jit(solution)/shard_map/ppermute | solution.py:123
  63.8 8.3 %collective-permute-start.5 = (bf16[12,16,256]{2,1,0:T(8,128)(2,1)S(1)}, bf16[12,16,256]{2,1,0:T(8,128)(2,1)S(1)}, u32[]{:S(2)}, u32[]{:S(2)}) collective-permute-start(bf16[12,16,256]{2,1,0:T(8,128)(2,1)S(1)} %slice.17), channel_id=1, source_target_pairs={{0,3},{1,0},{2,1},{3,2},{4,7},{5,4},{6,5},{7,6},{8,11},{9,8},{10,9... | collective-permute-start | bytes 294920 | tf_op jit(solution)/shard_map/ppermute | solution.py:130
  65.6 12.1 %collective-permute-start.7 = (bf16[20,16,256]{2,1,0:T(8,128)(2,1)S(1)}, bf16[20,16,256]{2,1,0:T(8,128)(2,1)S(1)}, u32[]{:S(2)}, u32[]{:S(2)}) collective-permute-start(bf16[20,16,256]{2,1,0:T(8,128)(2,1)S(1)} %slice.19), channel_id=1, source_target_pairs={{0,129},{1,130},{2,131},{3,128},{128,1},{129,2},{130,3},{131,0},{4... | collective-permute-start | bytes 491528 | tf_op jit(solution)/shard_map/ppermute | solution.py:129
  68.4 9.4 %collective-permute-start.4 = (bf16[20,16,256]{2,1,0:T(8,128)(2,1)S(1)}, bf16[20,16,256]{2,1,0:T(8,128)(2,1)S(1)}, u32[]{:S(2)}, u32[]{:S(2)}) collective-permute-start(bf16[20,16,256]{2,1,0:T(8,128)(2,1)S(1)} %slice.16), channel_id=1, source_target_pairs={{0,128},{128,0},{1,129},{129,1},{2,130},{130,2},{3,131},{131,3},{4... | collective-permute-start | bytes 491528 | tf_op jit(solution)/shard_map/ppermute | solution.py:128
  68.5 9.2 %collective-permute-start.8 = (bf16[32,16,256]{2,1,0:T(8,128)(2,1)S(1)}, bf16[32,16,256]{2,1,0:T(8,128)(2,1)S(1)}, u32[]{:S(2)}, u32[]{:S(2)}) collective-permute-start(bf16[32,16,256]{2,1,0:T(8,128)(2,1)S(1)} %collective-permute-done.3.refs_4_), channel_id=1, source_target_pairs={{0,1},{1,2},{2,3},{3,0},{4,5},{5,6},{6,7},{7,4},{8,9},{9,10},{10,1... | collective-permute-start | bytes 786440 | tf_op jit(solution)/shard_map/ppermute | solution.py:126
  69.1 8.6 %collective-permute-start.1 = (bf16[32,16,256]{2,1,0:T(8,128)(2,1)S(1)}, bf16[32,16,256]{2,1,0:T(8,128)(2,1)S(1)}, u32[]{:S(2)}, u32[]{:S(2)}) collective-permute-start(bf16[32,16,256]{2,1,0:T(8,128)(2,1)S(1)} %collective-permute-done.refs_1_), channel_id=1, source_target_pairs={{0,3},{1,0},{2,1},{3,2},{4,7},{5,4},{6,5},{7,6},{8,11},{9,8},{10,9... | collective-permute-start | bytes 786440 | tf_op jit(solution)/shard_map/ppermute | solution.py:127
  72.1 5.6 %collective-permute-start.6 = (bf16[12,16,256]{2,1,0:T(8,128)(2,1)S(1)}, bf16[12,16,256]{2,1,0:T(8,128)(2,1)S(1)}, u32[]{:S(2)}, u32[]{:S(2)}) collective-permute-start(bf16[12,16,256]{2,1,0:T(8,128)(2,1)S(1)} %slice.18), channel_id=1, source_target_pairs={{0,131},{1,128},{2,129},{3,130},{128,3},{129,0},{130,1},{131,2},{4... | collective-permute-start | bytes 294920 | tf_op jit(solution)/shard_map/ppermute | solution.py:131
  79.6 2.0 %collective-permute-start.9 = (bf16[16,96,128]{2,1,0:T(8,128)(2,1)S(1)}, bf16[16,96,128]{2,1,0:T(8,128)(2,1)S(1)}, u32[]{:S(2)}, u32[]{:S(2)}) collective-permute-start(bf16[16,96,128]{2,1,0:T(8,128)(2,1)S(1)} %get-tuple-element.16), channel_id=1, source_target_pairs={{0,4},{4,0},{1,5},{5,1},{2,6},{6,2},{3,7},{7,3},{8,12},{12,8},{9,1... | collective-permute-start | bytes 1179656 | tf_op jit(solution)/shard_map/ppermute | solution.py:160

commit v2 on v1

--- a/solution.py
+++ b/solution.py
@@ -30,6 +30,10 @@
     return lax.dot_general(a, b, (((1,), (1,)), ((), ())), preferred_element_type=jnp.float32)
 
 
+def from_both_ends(chips):
+    return [i // 2 if i % 2 == 0 else chips - 1 - i // 2 for i in range(chips)]
+
+
 def partial_sums(out, side, cores, active, down):
     shards, groups, quarter, width = down.shape
     rows, chips = groups * quarter, shards // cores
@@ -37,11 +41,14 @@
     none = jnp.zeros_like(tail)
     upper, lower = jnp.concatenate([tail, none]), jnp.concatenate([none, tail])
     weights = down.reshape(chips, cores, rows, width)[:, pl.ds(side, 1)][:, 0]
-    out[:, :rows] = nt_dot(weights.reshape(chips * rows, width), head).astype(out.dtype).reshape(chips, rows, LANES)
+    wide = nt_dot(weights.reshape(chips * rows, width), head).astype(out.dtype).reshape(chips, rows, LANES)
     packed = nt_dot(weights[:, : rows // 2].reshape(chips * rows // 2, width), upper) + nt_dot(
         weights[:, rows // 2 :].reshape(chips * rows // 2, width), lower
     )
-    out[:, rows:] = packed.astype(out.dtype).reshape(chips, rows // 2, LANES)
+    packed = packed.astype(out.dtype).reshape(chips, rows // 2, LANES)
+    for place, chip in enumerate(from_both_ends(chips)):
+        out[place, :rows] = wide[chip]
+        out[place, rows:] = packed[chip]
 
 
 def feed_forward(cores, where, normed, *refs):
@@ -158,7 +165,8 @@
         name="own_side",
     )(where, active, up, down)
     swapped = lax.ppermute(away, "core", ring(cores, 1))
-    arrived = lax.all_to_all(added(kept, swapped), "z", 0, 0, tiled=True)
+    order = [from_both_ends(chips)]
+    arrived = lax.all_to_all(added(kept, swapped), "z", 0, 0, axis_index_groups=order, tiled=True)
     out = pl.pallas_call(
         summed_up,
         out_shape=jax.ShapeDtypeStruct((rows_local, count), jnp.bfloat16),

time: 115 us -> 117 us (1.017)
  blocking collectives: 84.9 us -> 87.4 us
    all_to_all x1, blocking collectives: 31.4 us -> 33.9 us  [local(): lax.all_to_all(added(kept, swapped), 'z', 0, 0, axis_index_groups=order,...]
where the time goes in v2:
time: 117 us; the launch traced here: 116 us
  blocking collectives  87.4 us (75%)
  starting transfers between devices  13 us (11%)
  waiting for transfers between devices  8.58 us (7%)
  Pallas kernels  4.44 us (4%)
  other arithmetic  1.94 us (2%)
    all_to_all x1, blocking collectives, local(): lax.all_to_all(moved, 'z', 0, 0, tiled=True).reshape(shards, quarter, width)  42.1 us
    all_to_all x1, blocking collectives, local(): lax.all_to_all(added(kept, swapped), 'z', 0, 0, axis_index_groups=order,...  33.9 us
    all_to_all x1, blocking collectives, local(): moved = lax.all_to_all(pieces, ('core', 'tp'), 0, 0, tiled=True)  11.4 us
    ppermute x1, waiting for transfers between devices, local(): twin = lax.ppermute(own, 'member', ring(PAIR, 1))  4.58 us
    ppermute x1, starting transfers between devices, local(): lax.ppermute(left[:far_cut], ('member', 'tp'), across(groups, -1))  2.86 us
    ppermute x1, starting transfers between devices, local(): far = lax.ppermute(left, 'tp', ring(groups, -1))  2.77 us
    ppermute x1, starting transfers between devices, local(): lax.ppermute(right[far_cut:], ('member', 'tp'), across(groups, 1))  2.76 us
    ppermute x1, waiting for transfers between devices, local(): lax.ppermute(left[:far_cut], ('member', 'tp'), across(groups, -1))  2.69 us
  transfers between devices with their start and end apart: 10, of which 3 were waited for; matrix products, arithmetic and copies ran while one was open for 0% of the time, Pallas kernels for 2%

profile of v2, /device:TPU:40, one launch (start us, length us, event | category | flops | bytes accessed | tf_op | source)
XLA Modules:
  0.0 116.4 jit_solution(16666899588271520875)
XLA Ops:
  0.6 1.3 %select_convert_fusion = bf16[64,2048]{1,0:T(8,128)(2,1)S(1)} fusion(f32[64,2048]{1,0:T(8,128)} %param.7, f32[64,2048]{1,0:T(8,128)} %param.6, f32[64]{0:T(128)} %param.5, pred[]{:T(512)S(6)} %eq.3), kind=kLoop, calls=%fused_computation.5 | loop fusion | flops 262144 | bytes 1310977 | tf_op jit(solution)/shard_map/convert_element_type | solution.py:119
  2.0 0.2 reshape.33
  2.2 11.4 %all_to_all.15 = bf16[8,4,16,256]{3,2,1,0:T(8,128)(2,1)S(1)} all-to-all(bf16[8,4,16,256]{3,2,1,0:T(8,128)(2,1)S(1)} %bitcast.17), channel_id=1, replica_groups=mesh['pair'=1,'member'=2,'z'=16,'core'=2,'tp'=4] {'core','tp'}, dimensions={0} | all-to-all | bytes 524288 | tf_op jit(solution)/shard_map/all_to_all | solution.py:122
  13.6 42.1 %all_to_all.16 = bf16[16,2,16,256]{3,2,1,0:T(8,128)(2,1)S(1)} all-to-all(bf16[16,2,16,256]{3,2,1,0:T(8,128)(2,1)S(1)} %copy.11), channel_id=1, replica_groups=mesh['pair'=1,'member'=2,'z'=16,'core'=2,'tp'=4] {'z'}, dimensions={0} | all-to-all | bytes 524288 | tf_op jit(solution)/shard_map/all_to_all | solution.py:124
  55.7 0.9 collective-permute-start.2
  56.6 2.4 %collective-permute-start = (bf16[32,16,256]{2,1,0:T(8,128)(2,1)S(1)}, bf16[32,16,256]{2,1,0:T(8,128)(2,1)S(1)}, u32[]{:S(2)}, u32[]{:S(2)}) collective-permute-start(bf16[32,16,256]{2,1,0:T(8,128)(2,1)S(1)} %bitcast.14), channel_id=1, source_target_pairs={{0,3},{1,0},{2,1},{3,2},{4,7},{5,4},{6,5},{7,6},{8,11},{9,8},{10,9... | collective-permute-start | bytes 786440 | tf_op jit(solution)/shard_map/ppermute | solution.py:130
  59.0 0.2 fusion
  59.2 4.6 %collective-permute-done.3.refs_4_ = bf16[32,16,256]{2,1,0:T(8,128)(2,1)S(1)} collective-permute-done((bf16[32,16,256]{2,1,0:T(8,128)(2,1)S(1)}, bf16[32,16,256]{2,1,0:T(8,128)(2,1)S(1)}, u32[]{:S(2)}, u32[]{:S(2)}) %collective-permute-start.3) | collective-permute-done | bytes 262176 | tf_op jit(solution)/shard_map/ppermute | solution.py:129
  63.8 0.5 collective-permute-start.5
  64.3 1.3 %collective-permute-done.2.refs_3_ = bf16[32,16,256]{2,1,0:T(8,128)(2,1)S(1)} collective-permute-done((bf16[32,16,256]{2,1,0:T(8,128)(2,1)S(1)}, bf16[32,16,256]{2,1,0:T(8,128)(2,1)S(1)}, u32[]{:S(2)}, u32[]{:S(2)}) %collective-permute-start.2) | collective-permute-done | bytes 262176 | tf_op jit(solution)/shard_map/ppermute | solution.py:131
  65.6 2.8 %collective-permute-start.7 = (bf16[20,16,256]{2,1,0:T(8,128)(2,1)S(1)}, bf16[20,16,256]{2,1,0:T(8,128)(2,1)S(1)}, u32[]{:S(2)}, u32[]{:S(2)}) collective-permute-start(bf16[20,16,256]{2,1,0:T(8,128)(2,1)S(1)} %slice.19), channel_id=1, source_target_pairs={{0,129},{1,130},{2,131},{3,128},{128,1},{129,2},{130,3},{131,0},{4... | collective-permute-start | bytes 491528 | tf_op jit(solution)/shard_map/ppermute | solution.py:136
  68.4 0.1 collective-permute-start.4
  68.5 0.6 collective-permute-start.8
  69.1 2.8 %collective-permute-start.1 = (bf16[32,16,256]{2,1,0:T(8,128)(2,1)S(1)}, bf16[32,16,256]{2,1,0:T(8,128)(2,1)S(1)}, u32[]{:S(2)}, u32[]{:S(2)}) collective-permute-start(bf16[32,16,256]{2,1,0:T(8,128)(2,1)S(1)} %collective-permute-done.refs_1_), channel_id=1, source_target_pairs={{0,3},{1,0},{2,1},{3,2},{4,7},{5,4},{6,5},{7,6},{8,11},{9,8},{10,9... | collective-permute-start | bytes 786440 | tf_op jit(solution)/shard_map/ppermute | solution.py:134
  71.9 0.2 fusion.1.normed
  72.1 2.9 %collective-permute-start.6 = (bf16[12,16,256]{2,1,0:T(8,128)(2,1)S(1)}, bf16[12,16,256]{2,1,0:T(8,128)(2,1)S(1)}, u32[]{:S(2)}, u32[]{:S(2)}) collective-permute-start(bf16[12,16,256]{2,1,0:T(8,128)(2,1)S(1)} %slice.18), channel_id=1, source_target_pairs={{0,131},{1,128},{2,129},{3,130},{128,3},{129,0},{130,1},{131,2},{4... | collective-permute-start | bytes 294920 | tf_op jit(solution)/shard_map/ppermute | solution.py:138
  75.0 0.1 pad_add_fusion.where
  75.0 2.7 %collective-permute-done.6.refs_7_ = bf16[12,16,256]{2,1,0:T(8,128)(2,1)S(1)} collective-permute-done((bf16[12,16,256]{2,1,0:T(8,128)(2,1)S(1)}, bf16[12,16,256]{2,1,0:T(8,128)(2,1)S(1)}, u32[]{:S(2)}, u32[]{:S(2)}) %collective-permute-start.6) | collective-permute-done | bytes 98336 | tf_op jit(solution)/shard_map/ppermute | solution.py:138
  77.7 1.8 %feed_forward.1 = (bf16[32,4,16,256]{3,2,1,0:T(8,128)(2,1)S(1)}, bf16[32,4,16,256]{3,2,1,0:T(8,128)(2,1)S(1)}, bf16[192,256]{1,0:T(8,128)(2,1)S(1)}, bf16[16,96,128]{2,1,0:T(8,128)(2,1)S(1)}) custom-call(s32[3]{0:T(128)S(1)} %pad_add_fusion.where, bf16[192,2048]{1,0:T(8,128)(2,1)S(1)} %fusion.1.normed, bf16[32,16,256]{2,1,0:T(8,128)(2,1)S(1)} %bitcast.15, ...), custom_call_target="tpu_custom_call" | custom-call | flops 301989888 | bytes 4194304 | tf_op jit(solution)/shard_map/feed_forward/pallas_call | solution.py:141
  79.6 0.1 collective-permute-start.9
  79.7 1.9 %own_side.1 = (bf16[32,4,16,256]{3,2,1,0:T(8,128)(2,1)}, bf16[32,4,16,256]{3,2,1,0:T(8,128)(2,1)}, bf16[16,96,128]{2,1,0:T(8,128)(2,1)S(1)}) custom-call(s32[3]{0:T(128)S(1)} %pad_add_fusion.where, bf16[192,256]{1,0:T(8,128)(2,1)S(1)} %get-tuple-element.10.active, bf16[32,4,16,256]{3,2,1,0:T(8,128)(2,1)S(1)} %get-tuple-element.11.up, ...), custom_call_target="tpu_custom_call" | custom-call | flops 100663296 | bytes 4194304 | tf_op jit(solution)/shard_map/own_side/pallas_call | solution.py:155
  81.6 0.1 add_convert_fusion
  81.8 33.9 %all_to_all.17.arrived = bf16[16,96,128]{2,1,0:T(8,128)(2,1)S(1)} all-to-all(bf16[16,96,128]{2,1,0:T(8,128)(2,1)S(1)} %add_convert_fusion), channel_id=1, replica_groups={{0,120,8,112,16,104,24,96,32,88,40,80,48,72,56,64},{1,121,9,113,17,105,..., dimensions={0} | all-to-all | bytes 786432 | tf_op jit(solution)/shard_map/all_to_all | solution.py:169
  115.7 0.7 summed_up.1
  (17 shorter events, 0.1 us)
Async XLA Ops:
  2.1 56.8 %copy-start = (bf16[192,2048]{1,0:T(8,128)(2,1)S(1)}, bf16[192,2048]{1,0:T(8,128)(2,1)}, u32[]{:S(2)}) copy-start(bf16[192,2048]{1,0:T(8,128)(2,1)} %param.4) | copy-start | bytes 2359300
  55.7 8.1 %collective-permute-start.3 = (bf16[32,16,256]{2,1,0:T(8,128)(2,1)S(1)}, bf16[32,16,256]{2,1,0:T(8,128)(2,1)S(1)}, u32[]{:S(2)}, u32[]{:S(2)}) collective-permute-start(bf16[32,16,256]{2,1,0:T(8,128)(2,1)S(1)} %bitcast.12), channel_id=1, source_target_pairs={{0,128},{128,0},{1,129},{129,1},{2,130},{130,2},{3,131},{131,3},{4... | collective-permute-start | bytes 786440 | tf_op jit(solution)/shard_map/ppermute | solution.py:129
  55.7 9.8 %collective-permute-start.2 = (bf16[32,16,256]{2,1,0:T(8,128)(2,1)S(1)}, bf16[32,16,256]{2,1,0:T(8,128)(2,1)S(1)}, u32[]{:S(2)}, u32[]{:S(2)}) collective-permute-start(bf16[32,16,256]{2,1,0:T(8,128)(2,1)S(1)} %bitcast.13), channel_id=1, source_target_pairs={{0,1},{1,2},{2,3},{3,0},{4,5},{5,6},{6,7},{7,4},{8,9},{9,10},{10,1... | collective-permute-start | bytes 786440 | tf_op jit(solution)/shard_map/ppermute | solution.py:131
  56.6 11.8 %collective-permute-start = (bf16[32,16,256]{2,1,0:T(8,128)(2,1)S(1)}, bf16[32,16,256]{2,1,0:T(8,128)(2,1)S(1)}, u32[]{:S(2)}, u32[]{:S(2)}) collective-permute-start(bf16[32,16,256]{2,1,0:T(8,128)(2,1)S(1)} %bitcast.14), channel_id=1, source_target_pairs={{0,3},{1,0},{2,1},{3,2},{4,7},{5,4},{6,5},{7,6},{8,11},{9,8},{10,9... | collective-permute-start | bytes 786440 | tf_op jit(solution)/shard_map/ppermute | solution.py:130
  63.8 8.3 %collective-permute-start.5 = (bf16[12,16,256]{2,1,0:T(8,128)(2,1)S(1)}, bf16[12,16,256]{2,1,0:T(8,128)(2,1)S(1)}, u32[]{:S(2)}, u32[]{:S(2)}) collective-permute-start(bf16[12,16,256]{2,1,0:T(8,128)(2,1)S(1)} %slice.17), channel_id=1, source_target_pairs={{0,3},{1,0},{2,1},{3,2},{4,7},{5,4},{6,5},{7,6},{8,11},{9,8},{10,9... | collective-permute-start | bytes 294920 | tf_op jit(solution)/shard_map/ppermute | solution.py:137
  65.6 12.1 %collective-permute-start.7 = (bf16[20,16,256]{2,1,0:T(8,128)(2,1)S(1)}, bf16[20,16,256]{2,1,0:T(8,128)(2,1)S(1)}, u32[]{:S(2)}, u32[]{:S(2)}) collective-permute-start(bf16[20,16,256]{2,1,0:T(8,128)(2,1)S(1)} %slice.19), channel_id=1, source_target_pairs={{0,129},{1,130},{2,131},{3,128},{128,1},{129,2},{130,3},{131,0},{4... | collective-permute-start | bytes 491528 | tf_op jit(solution)/shard_map/ppermute | solution.py:136
  68.4 9.4 %collective-permute-start.4 = (bf16[20,16,256]{2,1,0:T(8,128)(2,1)S(1)}, bf16[20,16,256]{2,1,0:T(8,128)(2,1)S(1)}, u32[]{:S(2)}, u32[]{:S(2)}) collective-permute-start(bf16[20,16,256]{2,1,0:T(8,128)(2,1)S(1)} %slice.16), channel_id=1, source_target_pairs={{0,128},{128,0},{1,129},{129,1},{2,130},{130,2},{3,131},{131,3},{4... | collective-permute-start | bytes 491528 | tf_op jit(solution)/shard_map/ppermute | solution.py:135
  68.5 9.2 %collective-permute-start.8 = (bf16[32,16,256]{2,1,0:T(8,128)(2,1)S(1)}, bf16[32,16,256]{2,1,0:T(8,128)(2,1)S(1)}, u32[]{:S(2)}, u32[]{:S(2)}) collective-permute-start(bf16[32,16,256]{2,1,0:T(8,128)(2,1)S(1)} %collective-permute-done.3.refs_4_), channel_id=1, source_target_pairs={{0,1},{1,2},{2,3},{3,0},{4,5},{5,6},{6,7},{7,4},{8,9},{9,10},{10,1... | collective-permute-start | bytes 786440 | tf_op jit(solution)/shard_map/ppermute | solution.py:133
  69.1 8.6 %collective-permute-start.1 = (bf16[32,16,256]{2,1,0:T(8,128)(2,1)S(1)}, bf16[32,16,256]{2,1,0:T(8,128)(2,1)S(1)}, u32[]{:S(2)}, u32[]{:S(2)}) collective-permute-start(bf16[32,16,256]{2,1,0:T(8,128)(2,1)S(1)} %collective-permute-done.refs_1_), channel_id=1, source_target_pairs={{0,3},{1,0},{2,1},{3,2},{4,7},{5,4},{6,5},{7,6},{8,11},{9,8},{10,9... | collective-permute-start | bytes 786440 | tf_op jit(solution)/shard_map/ppermute | solution.py:134
  72.1 5.6 %collective-permute-start.6 = (bf16[12,16,256]{2,1,0:T(8,128)(2,1)S(1)}, bf16[12,16,256]{2,1,0:T(8,128)(2,1)S(1)}, u32[]{:S(2)}, u32[]{:S(2)}) collective-permute-start(bf16[12,16,256]{2,1,0:T(8,128)(2,1)S(1)} %slice.18), channel_id=1, source_target_pairs={{0,131},{1,128},{2,129},{3,130},{128,3},{129,0},{130,1},{131,2},{4... | collective-permute-start | bytes 294920 | tf_op jit(solution)/shard_map/ppermute | solution.py:138
  79.6 2.0 %collective-permute-start.9 = (bf16[16,96,128]{2,1,0:T(8,128)(2,1)S(1)}, bf16[16,96,128]{2,1,0:T(8,128)(2,1)S(1)}, u32[]{:S(2)}, u32[]{:S(2)}) collective-permute-start(bf16[16,96,128]{2,1,0:T(8,128)(2,1)S(1)} %get-tuple-element.16), channel_id=1, source_target_pairs={{0,4},{4,0},{1,5},{5,1},{2,6},{6,2},{3,7},{7,3},{8,12},{12,8},{9,1... | collective-permute-start | bytes 1179656 | tf_op jit(solution)/shard_map/ppermute | solution.py:167

commit v3 on v1

--- a/solution.py
+++ b/solution.py
@@ -30,24 +30,29 @@
     return lax.dot_general(a, b, (((1,), (1,)), ((), ())), preferred_element_type=jnp.float32)
 
 
-def partial_sums(out, side, cores, active, down):
+def partial_sums(out, parity, side, cores, active, down):
     shards, groups, quarter, width = down.shape
-    rows, chips = groups * quarter, shards // cores
+    rows, blocks = groups * quarter, shards // cores // 2
     head, tail = active[:LANES], active[LANES:]
     none = jnp.zeros_like(tail)
     upper, lower = jnp.concatenate([tail, none]), jnp.concatenate([none, tail])
-    weights = down.reshape(chips, cores, rows, width)[:, pl.ds(side, 1)][:, 0]
-    out[:, :rows] = nt_dot(weights.reshape(chips * rows, width), head).astype(out.dtype).reshape(chips, rows, LANES)
-    packed = nt_dot(weights[:, : rows // 2].reshape(chips * rows // 2, width), upper) + nt_dot(
-        weights[:, rows // 2 :].reshape(chips * rows // 2, width), lower
-    )
-    out[:, rows:] = packed.astype(out.dtype).reshape(chips, rows // 2, LANES)
+    for part in (1, 0):
+        on = lax.rem(parity + part, 2) * cores + side
+        weights = down.reshape(blocks, 2 * cores, rows, width)[:, pl.ds(on, 1)][:, 0]
+        wide = nt_dot(weights.reshape(blocks * rows, width), head).astype(out.dtype).reshape(blocks, rows, LANES)
+        packed = nt_dot(weights[:, : rows // 2].reshape(blocks * rows // 2, width), upper) + nt_dot(
+            weights[:, rows // 2 :].reshape(blocks * rows // 2, width), lower
+        )
+        packed = packed.astype(out.dtype).reshape(blocks, rows // 2, LANES)
+        for block in range(blocks):
+            out[part, blocks - 1 - block, :rows] = wide[block]
+            out[part, blocks - 1 - block, rows:] = packed[block]
 
 
 def feed_forward(cores, where, normed, *refs):
     quarters, (up, down, active, away) = refs[:-4], refs[-4:]
     shards, groups, quarter, width = up.shape
-    at, core, member = where[0], where[1], where[2]
+    at, core, member, parity = where[0], where[1], where[2], where[3]
 
     def place(weight, *pieces):
         for step, parts in enumerate(pieces):
@@ -70,14 +75,14 @@
     )
     rounded = jnp.square(jnp.maximum(hidden, 0.0)).astype(active.dtype)
     active[...] = rounded
-    partial_sums(away, 1 - core, cores, rounded, down)
+    partial_sums(away, parity, 1 - core, cores, rounded, down)
 
 
 def own_side(cores, where, active, up, down, up_out, down_out, kept, sems):
     writes = [pltpu.make_async_copy(up, up_out, sems.at[0]), pltpu.make_async_copy(down, down_out, sems.at[1])]
     for write in writes:
         write.start()
-    partial_sums(kept, where[1], cores, active[...], down)
+    partial_sums(kept, where[3], where[1], cores, active[...], down)
     for write in writes:
         write.wait()
 
@@ -106,7 +111,7 @@
     width = cols_local * groups // shards
     blocks = cols_local // (width * cores)
     quarter = rows_local // groups
-    where = jnp.stack([lax.axis_index("tp"), lax.axis_index("core"), lax.axis_index("member")]).astype(jnp.int32)
+    where = jnp.stack([lax.axis_index("tp"), lax.axis_index("core"), lax.axis_index("member"), lax.axis_index("z") % 2]).astype(jnp.int32)
     smem, vmem = pl.BlockSpec(memory_space=pltpu.SMEM), pl.BlockSpec(memory_space=pltpu.VMEM)
     first = lax.axis_index("member") == 0
     mine = jnp.where(first, norm_gain[:, None] * up_trained, down_trained).astype(jnp.bfloat16)
@@ -130,7 +135,7 @@
     twin_left_second = lax.ppermute(twin[cut:], "tp", ring(groups, -1))
     twin_far_first = lax.ppermute(left[:far_cut], ("member", "tp"), across(groups, -1))
     served = jax.ShapeDtypeStruct((shards, groups, quarter, width), jnp.bfloat16)
-    part = jax.ShapeDtypeStruct((chips, rows_local * count // LANES, LANES), jnp.bfloat16)
+    part = jax.ShapeDtypeStruct((2, chips // 2, rows_local * count // LANES, LANES), jnp.bfloat16)
     up, down, active, away = pl.pallas_call(
         functools.partial(feed_forward, cores),
         out_shape=[served, served, jax.ShapeDtypeStruct((count, width), jnp.bfloat16), part],
@@ -158,7 +163,13 @@
         name="own_side",
     )(where, active, up, down)
     swapped = lax.ppermute(away, "core", ring(cores, 1))
-    arrived = lax.all_to_all(added(kept, swapped), "z", 0, 0, tiled=True)
+    leaving = added(kept[1], swapped[1])
+    mid = chips // 4
+    up_one = lax.ppermute(leaving[:mid], "z", ring(chips, 1))
+    down_one = lax.ppermute(leaving[mid:], "z", ring(chips, -1))
+    summed = added(added(kept[0], swapped[0]), jnp.concatenate([up_one, down_one]))
+    same_parity = [list(range(chips - 2 + first, -1, -2)) for first in range(2)]
+    arrived = lax.all_to_all(summed, "z", 0, 0, axis_index_groups=same_parity, tiled=True)
     out = pl.pallas_call(
         summed_up,
         out_shape=jax.ShapeDtypeStruct((rows_local, count), jnp.bfloat16),

time: 115 us -> 113 us (0.983)
  the two profiles are of different devices: /device:TPU:40 before, /device:TPU:160 now
where the time goes in v3:
time: 113 us; the launch traced here: 112 us
  blocking collectives  77.4 us (68%)
  starting transfers between devices  16.5 us (15%)
  waiting for transfers between devices  11.1 us (10%)
  Pallas kernels  4.42 us (4%)
  other arithmetic  1.82 us (2%)
    all_to_all x1, blocking collectives, local(): lax.all_to_all(moved, 'z', 0, 0, tiled=True).reshape(shards, quarter, width)  41.1 us
    all_to_all x1, blocking collectives, local(): lax.all_to_all(summed, 'z', 0, 0, axis_index_groups=same_parity, tiled=True)  25 us
    all_to_all x1, blocking collectives, local(): moved = lax.all_to_all(pieces, ('core', 'tp'), 0, 0, tiled=True)  11.4 us
    ppermute x1, waiting for transfers between devices, local(): up_one = lax.ppermute(leaving[:mid], 'z', ring(chips, 1))  3.16 us
    ppermute x1, starting transfers between devices, local(): far = lax.ppermute(left, 'tp', ring(groups, -1))  2.9 us
    ppermute x1, starting transfers between devices, local(): lax.ppermute(left[:far_cut], ('member', 'tp'), across(groups, -1))  2.78 us
    ppermute x1, waiting for transfers between devices, local(): lax.ppermute(left[:far_cut], ('member', 'tp'), across(groups, -1))  2.77 us
    ppermute x1, starting transfers between devices, local(): left = lax.ppermute(own, 'tp', ring(groups, -1))  2.38 us
  transfers between devices with their start and end apart: 12, of which 6 were waited for; matrix products, arithmetic and copies ran while one was open for 0% of the time, Pallas kernels for 2%

profile of v3, /device:TPU:160, one launch (start us, length us, event | category | flops | bytes accessed | tf_op | source)
XLA Modules:
  0.0 112.4 jit_solution(6690012014060634998)
XLA Ops:
  0.6 1.2 %select_convert_fusion = bf16[64,2048]{1,0:T(8,128)(2,1)S(1)} fusion(f32[64,2048]{1,0:T(8,128)} %param.7, f32[64,2048]{1,0:T(8,128)} %param.6, f32[64]{0:T(128)} %param.5, pred[]{:T(512)S(6)} %eq.5), kind=kLoop, calls=%fused_computation.4 | loop fusion | flops 262144 | bytes 1310977 | tf_op jit(solution)/shard_map/convert_element_type | solution.py:117
  2.1 11.4 %all_to_all.15 = bf16[8,4,16,256]{3,2,1,0:T(8,128)(2,1)S(1)} all-to-all(bf16[8,4,16,256]{3,2,1,0:T(8,128)(2,1)S(1)} %bitcast.27), channel_id=1, replica_groups=mesh['pair'=1,'member'=2,'z'=16,'core'=2,'tp'=4] {'core','tp'}, dimensions={0} | all-to-all | bytes 524288 | tf_op jit(solution)/shard_map/all_to_all | solution.py:120
  13.5 41.1 %all_to_all.16 = bf16[16,2,16,256]{3,2,1,0:T(8,128)(2,1)S(1)} all-to-all(bf16[16,2,16,256]{3,2,1,0:T(8,128)(2,1)S(1)} %copy.11), channel_id=1, replica_groups=mesh['pair'=1,'member'=2,'z'=16,'core'=2,'tp'=4] {'z'}, dimensions={0} | all-to-all | bytes 524288 | tf_op jit(solution)/shard_map/all_to_all | solution.py:122
  54.6 2.3 %collective-permute-start.3 = (bf16[32,16,256]{2,1,0:T(8,128)(2,1)S(1)}, bf16[32,16,256]{2,1,0:T(8,128)(2,1)S(1)}, u32[]{:S(2)}, u32[]{:S(2)}) collective-permute-start(bf16[32,16,256]{2,1,0:T(8,128)(2,1)S(1)} %bitcast.22), channel_id=1, source_target_pairs={{0,128},{128,0},{1,129},{129,1},{2,130},{130,2},{3,131},{131,3},{4... | collective-permute-start | bytes 786440 | tf_op jit(solution)/shard_map/ppermute | solution.py:127
  56.9 0.9 collective-permute-start.2
  57.7 2.4 %collective-permute-start = (bf16[32,16,256]{2,1,0:T(8,128)(2,1)S(1)}, bf16[32,16,256]{2,1,0:T(8,128)(2,1)S(1)}, u32[]{:S(2)}, u32[]{:S(2)}) collective-permute-start(bf16[32,16,256]{2,1,0:T(8,128)(2,1)S(1)} %bitcast.24), channel_id=1, source_target_pairs={{0,3},{1,0},{2,1},{3,2},{4,7},{5,4},{6,5},{7,6},{8,11},{9,8},{10,9... | collective-permute-start | bytes 786440 | tf_op jit(solution)/shard_map/ppermute | solution.py:128
  60.1 0.2 fusion
  60.3 2.2 %collective-permute-done.3.refs_4_ = bf16[32,16,256]{2,1,0:T(8,128)(2,1)S(1)} collective-permute-done((bf16[32,16,256]{2,1,0:T(8,128)(2,1)S(1)}, bf16[32,16,256]{2,1,0:T(8,128)(2,1)S(1)}, u32[]{:S(2)}, u32[]{:S(2)}) %collective-permute-start.3) | collective-permute-done | bytes 262176 | tf_op jit(solution)/shard_map/ppermute | solution.py:127
  62.5 1.0 collective-permute-start.5
  63.6 1.7 %collective-permute-done.2.refs_3_ = bf16[32,16,256]{2,1,0:T(8,128)(2,1)S(1)} collective-permute-done((bf16[32,16,256]{2,1,0:T(8,128)(2,1)S(1)}, bf16[32,16,256]{2,1,0:T(8,128)(2,1)S(1)}, u32[]{:S(2)}, u32[]{:S(2)}) %collective-permute-start.2) | collective-permute-done | bytes 262176 | tf_op jit(solution)/shard_map/ppermute | solution.py:129
  65.2 0.8 collective-permute-start.7
  66.0 0.6 collective-permute-start.4
  66.6 0.7 collective-permute-start.8
  67.3 2.9 %collective-permute-start.1 = (bf16[32,16,256]{2,1,0:T(8,128)(2,1)S(1)}, bf16[32,16,256]{2,1,0:T(8,128)(2,1)S(1)}, u32[]{:S(2)}, u32[]{:S(2)}) collective-permute-start(bf16[32,16,256]{2,1,0:T(8,128)(2,1)S(1)} %collective-permute-done.refs_1_), channel_id=1, source_target_pairs={{0,3},{1,0},{2,1},{3,2},{4,7},{5,4},{6,5},{7,6},{8,11},{9,8},{10,9... | collective-permute-start | bytes 786440 | tf_op jit(solution)/shard_map/ppermute | solution.py:132
  70.2 0.2 fusion.1.normed
  70.4 2.8 %collective-permute-start.6 = (bf16[12,16,256]{2,1,0:T(8,128)(2,1)S(1)}, bf16[12,16,256]{2,1,0:T(8,128)(2,1)S(1)}, u32[]{:S(2)}, u32[]{:S(2)}) collective-permute-start(bf16[12,16,256]{2,1,0:T(8,128)(2,1)S(1)} %slice.50), channel_id=1, source_target_pairs={{0,131},{1,128},{2,129},{3,130},{128,3},{129,0},{130,1},{131,2},{4... | collective-permute-start | bytes 294920 | tf_op jit(solution)/shard_map/ppermute | solution.py:136
  73.3 2.8 %collective-permute-done.6.refs_7_ = bf16[12,16,256]{2,1,0:T(8,128)(2,1)S(1)} collective-permute-done((bf16[12,16,256]{2,1,0:T(8,128)(2,1)S(1)}, bf16[12,16,256]{2,1,0:T(8,128)(2,1)S(1)}, u32[]{:S(2)}, u32[]{:S(2)}) %collective-permute-start.6) | collective-permute-done | bytes 98336 | tf_op jit(solution)/shard_map/ppermute | solution.py:136
  76.1 1.2 %collective-permute-done.8.refs_9_ = bf16[32,16,256]{2,1,0:T(8,128)(2,1)S(1)} collective-permute-done((bf16[32,16,256]{2,1,0:T(8,128)(2,1)S(1)}, bf16[32,16,256]{2,1,0:T(8,128)(2,1)S(1)}, u32[]{:S(2)}, u32[]{:S(2)}) %collective-permute-start.8) | collective-permute-done | bytes 262176 | tf_op jit(solution)/shard_map/ppermute | solution.py:131
  77.3 1.8 %feed_forward.1 = (bf16[32,4,16,256]{3,2,1,0:T(8,128)(2,1)S(1)}, bf16[32,4,16,256]{3,2,1,0:T(8,128)(2,1)S(1)}, bf16[192,256]{1,0:T(8,128)(2,1)S(1)}, bf16[2,8,96,128]{3,2,1,0:T(8,128)(2,1)S(1)}) custom-call(s32[4]{0:T(128)S(1)} %pad_add_fusion.where, bf16[192,2048]{1,0:T(8,128)(2,1)S(1)} %fusion.1.normed, bf16[32,16,256]{2,1,0:T(8,128)(2,1)S(1)} %bitcast.25, ...), custom_call_target="tpu_custom_call" | custom-call | flops 301989888 | bytes 4194304 | tf_op jit(solution)/shard_map/feed_forward/pallas_call | solution.py:139
  79.2 1.9 %own_side.1 = (bf16[32,4,16,256]{3,2,1,0:T(8,128)(2,1)}, bf16[32,4,16,256]{3,2,1,0:T(8,128)(2,1)}, bf16[2,8,96,128]{3,2,1,0:T(8,128)(2,1)S(1)}) custom-call(s32[4]{0:T(128)S(1)} %pad_add_fusion.where, bf16[192,256]{1,0:T(8,128)(2,1)S(1)} %get-tuple-element.10.active, bf16[32,4,16,256]{3,2,1,0:T(8,128)(2,1)S(1)} %get-tuple-element.11.up, ...), custom_call_target="tpu_custom_call" | custom-call | flops 100663296 | bytes 4194304 | tf_op jit(solution)/shard_map/own_side/pallas_call | solution.py:153
  81.4 2.0 %collective-permute-start.11 = (bf16[4,96,128]{2,1,0:T(8,128)(2,1)S(1)}, bf16[4,96,128]{2,1,0:T(8,128)(2,1)S(1)}, u32[]{:S(2)}, u32[]{:S(2)}) collective-permute-start(bf16[4,96,128]{2,1,0:T(8,128)(2,1)S(1)} %get-tuple-element.18), channel_id=1, source_target_pairs={{0,120},{8,0},{16,8},{24,16},{32,24},{40,32},{48,40},{56,48},{64,5... | collective-permute-start | bytes 294920 | tf_op jit(solution)/shard_map/ppermute | solution.py:169
  83.4 3.2 %collective-permute-done.10 = bf16[4,96,128]{2,1,0:T(8,128)(2,1)S(1)} collective-permute-done((bf16[4,96,128]{2,1,0:T(8,128)(2,1)S(1)}, bf16[4,96,128]{2,1,0:T(8,128)(2,1)S(1)}, u32[]{:S(2)}, u32[]{:S(2)}) %collective-permute-start.10) | collective-permute-done | bytes 98336 | tf_op jit(solution)/shard_map/ppermute | solution.py:168
  86.8 25.0 %all_to_all.17.arrived = bf16[8,96,128]{2,1,0:T(8,128)(2,1)S(1)} all-to-all(bf16[8,96,128]{2,1,0:T(8,128)(2,1)S(1)} %fusion.2), channel_id=1, replica_groups={{112,96,80,64,48,32,16,0},{120,104,88,72,56,40,24,8},{113,97,81,65,49,3..., dimensions={0} | all-to-all | bytes 393216 | tf_op jit(solution)/shard_map/all_to_all | solution.py:172
  111.7 0.7 summed_up.1
  (23 shorter events, 1.0 us)
Async XLA Ops:
  2.0 58.1 %copy-start = (bf16[192,2048]{1,0:T(8,128)(2,1)S(1)}, bf16[192,2048]{1,0:T(8,128)(2,1)}, u32[]{:S(2)}) copy-start(bf16[192,2048]{1,0:T(8,128)(2,1)} %param.4) | copy-start | bytes 2359300
  54.6 8.0 %collective-permute-start.3 = (bf16[32,16,256]{2,1,0:T(8,128)(2,1)S(1)}, bf16[32,16,256]{2,1,0:T(8,128)(2,1)S(1)}, u32[]{:S(2)}, u32[]{:S(2)}) collective-permute-start(bf16[32,16,256]{2,1,0:T(8,128)(2,1)S(1)} %bitcast.22), channel_id=1, source_target_pairs={{0,128},{128,0},{1,129},{129,1},{2,130},{130,2},{3,131},{131,3},{4... | collective-permute-start | bytes 786440 | tf_op jit(solution)/shard_map/ppermute | solution.py:127
  56.9 8.4 %collective-permute-start.2 = (bf16[32,16,256]{2,1,0:T(8,128)(2,1)S(1)}, bf16[32,16,256]{2,1,0:T(8,128)(2,1)S(1)}, u32[]{:S(2)}, u32[]{:S(2)}) collective-permute-start(bf16[32,16,256]{2,1,0:T(8,128)(2,1)S(1)} %bitcast.23), channel_id=1, source_target_pairs={{0,1},{1,2},{2,3},{3,0},{4,5},{5,6},{6,7},{7,4},{8,9},{9,10},{10,1... | collective-permute-start | bytes 786440 | tf_op jit(solution)/shard_map/ppermute | solution.py:129
  57.7 8.3 %collective-permute-start = (bf16[32,16,256]{2,1,0:T(8,128)(2,1)S(1)}, bf16[32,16,256]{2,1,0:T(8,128)(2,1)S(1)}, u32[]{:S(2)}, u32[]{:S(2)}) collective-permute-start(bf16[32,16,256]{2,1,0:T(8,128)(2,1)S(1)} %bitcast.24), channel_id=1, source_target_pairs={{0,3},{1,0},{2,1},{3,2},{4,7},{5,4},{6,5},{7,6},{8,11},{9,8},{10,9... | collective-permute-start | bytes 786440 | tf_op jit(solution)/shard_map/ppermute | solution.py:128
  62.5 7.9 %collective-permute-start.5 = (bf16[12,16,256]{2,1,0:T(8,128)(2,1)S(1)}, bf16[12,16,256]{2,1,0:T(8,128)(2,1)S(1)}, u32[]{:S(2)}, u32[]{:S(2)}) collective-permute-start(bf16[12,16,256]{2,1,0:T(8,128)(2,1)S(1)} %slice.49), channel_id=1, source_target_pairs={{0,3},{1,0},{2,1},{3,2},{4,7},{5,4},{6,5},{7,6},{8,11},{9,8},{10,9... | collective-permute-start | bytes 294920 | tf_op jit(solution)/shard_map/ppermute | solution.py:135
  65.2 10.8 %collective-permute-start.7 = (bf16[20,16,256]{2,1,0:T(8,128)(2,1)S(1)}, bf16[20,16,256]{2,1,0:T(8,128)(2,1)S(1)}, u32[]{:S(2)}, u32[]{:S(2)}) collective-permute-start(bf16[20,16,256]{2,1,0:T(8,128)(2,1)S(1)} %slice.51), channel_id=1, source_target_pairs={{0,129},{1,130},{2,131},{3,128},{128,1},{129,2},{130,3},{131,0},{4... | collective-permute-start | bytes 491528 | tf_op jit(solution)/shard_map/ppermute | solution.py:134
  66.0 10.0 %collective-permute-start.4 = (bf16[20,16,256]{2,1,0:T(8,128)(2,1)S(1)}, bf16[20,16,256]{2,1,0:T(8,128)(2,1)S(1)}, u32[]{:S(2)}, u32[]{:S(2)}) collective-permute-start(bf16[20,16,256]{2,1,0:T(8,128)(2,1)S(1)} %slice.48), channel_id=1, source_target_pairs={{0,128},{128,0},{1,129},{129,1},{2,130},{130,2},{3,131},{131,3},{4... | collective-permute-start | bytes 491528 | tf_op jit(solution)/shard_map/ppermute | solution.py:133
  66.6 10.7 %collective-permute-start.8 = (bf16[32,16,256]{2,1,0:T(8,128)(2,1)S(1)}, bf16[32,16,256]{2,1,0:T(8,128)(2,1)S(1)}, u32[]{:S(2)}, u32[]{:S(2)}) collective-permute-start(bf16[32,16,256]{2,1,0:T(8,128)(2,1)S(1)} %collective-permute-done.3.refs_4_), channel_id=1, source_target_pairs={{0,1},{1,2},{2,3},{3,0},{4,5},{5,6},{6,7},{7,4},{8,9},{9,10},{10,1... | collective-permute-start | bytes 786440 | tf_op jit(solution)/shard_map/ppermute | solution.py:131
  67.3 10.0 %collective-permute-start.1 = (bf16[32,16,256]{2,1,0:T(8,128)(2,1)S(1)}, bf16[32,16,256]{2,1,0:T(8,128)(2,1)S(1)}, u32[]{:S(2)}, u32[]{:S(2)}) collective-permute-start(bf16[32,16,256]{2,1,0:T(8,128)(2,1)S(1)} %collective-permute-done.refs_1_), channel_id=1, source_target_pairs={{0,3},{1,0},{2,1},{3,2},{4,7},{5,4},{6,5},{7,6},{8,11},{9,8},{10,9... | collective-permute-start | bytes 786440 | tf_op jit(solution)/shard_map/ppermute | solution.py:132
  70.4 5.6 %collective-permute-start.6 = (bf16[12,16,256]{2,1,0:T(8,128)(2,1)S(1)}, bf16[12,16,256]{2,1,0:T(8,128)(2,1)S(1)}, u32[]{:S(2)}, u32[]{:S(2)}) collective-permute-start(bf16[12,16,256]{2,1,0:T(8,128)(2,1)S(1)} %slice.50), channel_id=1, source_target_pairs={{0,131},{1,128},{2,129},{3,130},{128,3},{129,0},{130,1},{131,2},{4... | collective-permute-start | bytes 294920 | tf_op jit(solution)/shard_map/ppermute | solution.py:136
  79.1 2.1 %collective-permute-start.9 = (bf16[2,8,96,128]{3,2,1,0:T(8,128)(2,1)S(1)}, bf16[2,8,96,128]{3,2,1,0:T(8,128)(2,1)S(1)}, u32[]{:S(2)}, u32[]{:S(2)}) collective-permute-start(bf16[2,8,96,128]{3,2,1,0:T(8,128)(2,1)S(1)} %get-tuple-element.16), channel_id=1, source_target_pairs={{0,4},{4,0},{1,5},{5,1},{2,6},{6,2},{3,7},{7,3},{8,12},{12,8},{9,1... | collective-permute-start | bytes 1179656 | tf_op jit(solution)/shard_map/ppermute | solution.py:165
  81.2 5.3 %collective-permute-start.10 = (bf16[4,96,128]{2,1,0:T(8,128)(2,1)S(1)}, bf16[4,96,128]{2,1,0:T(8,128)(2,1)S(1)}, u32[]{:S(2)}, u32[]{:S(2)}) collective-permute-start(bf16[4,96,128]{2,1,0:T(8,128)(2,1)S(1)} %get-tuple-element.17), channel_id=1, source_target_pairs={{0,8},{8,16},{16,24},{24,32},{32,40},{40,48},{48,56},{56,64},{64,7... | collective-permute-start | bytes 294920 | tf_op jit(solution)/shard_map/ppermute | solution.py:168
  81.4 5.3 %collective-permute-start.11 = (bf16[4,96,128]{2,1,0:T(8,128)(2,1)S(1)}, bf16[4,96,128]{2,1,0:T(8,128)(2,1)S(1)}, u32[]{:S(2)}, u32[]{:S(2)}) collective-permute-start(bf16[4,96,128]{2,1,0:T(8,128)(2,1)S(1)} %get-tuple-element.18), channel_id=1, source_target_pairs={{0,120},{8,0},{16,8},{24,16},{32,24},{40,32},{48,40},{56,48},{64,5... | collective-permute-start | bytes 294920 | tf_op jit(solution)/shard_map/ppermute | solution.py:169

commit v4 on v3

--- a/solution.py
+++ b/solution.py
@@ -28,6 +28,10 @@
 
 def nt_dot(a, b):
     return lax.dot_general(a, b, (((1,), (1,)), ((), ())), preferred_element_type=jnp.float32)
+
+
+def places(blocks, odd):
+    return [(blocks - 1 - (3 if odd else 1) * block) % blocks for block in range(blocks)]
 
 
 def partial_sums(out, parity, side, cores, active, down):
@@ -44,9 +48,11 @@
             weights[:, rows // 2 :].reshape(blocks * rows // 2, width), lower
         )
         packed = packed.astype(out.dtype).reshape(blocks, rows // 2, LANES)
-        for block in range(blocks):
-            out[part, blocks - 1 - block, :rows] = wide[block]
-            out[part, blocks - 1 - block, rows:] = packed[block]
+        odd = lax.rem(parity + part, 2)
+        for block, (even_place, odd_place) in enumerate(zip(places(blocks, False), places(blocks, True))):
+            place = pl.ds(jnp.where(odd == 0, even_place, odd_place), 1)
+            out[part, place, :rows] = wide[block][None]
+            out[part, place, rows:] = packed[block][None]
 
 
 def feed_forward(cores, where, normed, *refs):
@@ -127,7 +133,7 @@
     twin = lax.ppermute(own, "member", ring(PAIR, 1))
     left = lax.ppermute(own, "tp", ring(groups, -1))
     right = lax.ppermute(own, "tp", ring(groups, 1))
-    cut, far_cut = shards * 5 // 8, shards * 3 // 8
+    cut, far_cut = shards // 2, shards // 4
     twin_right = lax.ppermute(twin, "tp", ring(groups, 1))
     far = lax.ppermute(left, "tp", ring(groups, -1))
     twin_left_first = lax.ppermute(left[:cut], "member", ring(PAIR, 1))
@@ -168,7 +174,9 @@
     up_one = lax.ppermute(leaving[:mid], "z", ring(chips, 1))
     down_one = lax.ppermute(leaving[mid:], "z", ring(chips, -1))
     summed = added(added(kept[0], swapped[0]), jnp.concatenate([up_one, down_one]))
-    same_parity = [list(range(chips - 2 + first, -1, -2)) for first in range(2)]
+    same_parity = [
+        sorted(range(odd, chips, 2), key=lambda chip: places(chips // 2, odd)[chip // 2]) for odd in range(2)
+    ]
     arrived = lax.all_to_all(summed, "z", 0, 0, axis_index_groups=same_parity, tiled=True)
     out = pl.pallas_call(
         summed_up,

time: 113 us -> 113 us (level)
  the two profiles are of different devices: /device:TPU:160 before, /device:TPU:40 now
where the time goes in v4:
time: 113 us; the launch traced here: 112 us
  blocking collectives  74.6 us (66%)
  waiting for transfers between devices  16 us (14%)
  starting transfers between devices  13.7 us (12%)
  Pallas kernels  4.54 us (4%)
  other arithmetic  1.97 us (2%)
    all_to_all x1, blocking collectives, local(): lax.all_to_all(moved, 'z', 0, 0, tiled=True).reshape(shards, quarter, width)  42.1 us
    all_to_all x1, blocking collectives, local(): lax.all_to_all(summed, 'z', 0, 0, axis_index_groups=same_parity, tiled=True)  21.1 us
    all_to_all x1, blocking collectives, local(): moved = lax.all_to_all(pieces, ('core', 'tp'), 0, 0, tiled=True)  11.4 us
    ppermute x1, waiting for transfers between devices, local(): left = lax.ppermute(own, 'tp', ring(groups, -1))  6.94 us
    ppermute x1, starting transfers between devices, local(): far = lax.ppermute(left, 'tp', ring(groups, -1))  3.23 us
    ppermute x1, waiting for transfers between devices, local(): up_one = lax.ppermute(leaving[:mid], 'z', ring(chips, 1))  3.14 us
    ppermute x1, starting transfers between devices, local(): down_one = lax.ppermute(leaving[mid:], 'z', ring(chips, -1))  2.85 us
    ppermute x1, waiting for transfers between devices, local(): twin_right = lax.ppermute(twin, 'tp', ring(groups, 1))  2.68 us
  transfers between devices with their start and end apart: 12, of which 6 were waited for; matrix products, arithmetic and copies ran while one was open for 0% of the time, Pallas kernels for 2%

profile of v4, /device:TPU:40, one launch (start us, length us, event | category | flops | bytes accessed | tf_op | source)
XLA Modules:
  0.0 111.8 jit_solution(13711754152155224730)
XLA Ops:
  0.6 1.3 %select_convert_fusion = bf16[64,2048]{1,0:T(8,128)(2,1)S(1)} fusion(f32[64,2048]{1,0:T(8,128)} %param.7, f32[64,2048]{1,0:T(8,128)} %param.6, f32[64]{0:T(128)} %param.5, pred[]{:T(512)S(6)} %eq.5), kind=kLoop, calls=%fused_computation.4 | loop fusion | flops 262144 | bytes 1310977 | tf_op jit(solution)/shard_map/convert_element_type | solution.py:123
  2.2 11.4 %all_to_all.15 = bf16[8,4,16,256]{3,2,1,0:T(8,128)(2,1)S(1)} all-to-all(bf16[8,4,16,256]{3,2,1,0:T(8,128)(2,1)S(1)} %bitcast.27), channel_id=1, replica_groups=mesh['pair'=1,'member'=2,'z'=16,'core'=2,'tp'=4] {'core','tp'}, dimensions={0} | all-to-all | bytes 524288 | tf_op jit(solution)/shard_map/all_to_all | solution.py:126
  13.6 42.1 %all_to_all.16 = bf16[16,2,16,256]{3,2,1,0:T(8,128)(2,1)S(1)} all-to-all(bf16[16,2,16,256]{3,2,1,0:T(8,128)(2,1)S(1)} %copy.11), channel_id=1, replica_groups=mesh['pair'=1,'member'=2,'z'=16,'core'=2,'tp'=4] {'z'}, dimensions={0} | all-to-all | bytes 524288 | tf_op jit(solution)/shard_map/all_to_all | solution.py:128
  55.7 1.5 %collective-permute-start = (bf16[32,16,256]{2,1,0:T(8,128)(2,1)S(1)}, bf16[32,16,256]{2,1,0:T(8,128)(2,1)S(1)}, u32[]{:S(2)}, u32[]{:S(2)}) collective-permute-start(bf16[32,16,256]{2,1,0:T(8,128)(2,1)S(1)} %bitcast.22), channel_id=1, source_target_pairs={{0,3},{1,0},{2,1},{3,2},{4,7},{5,4},{6,5},{7,6},{8,11},{9,8},{10,9... | collective-permute-start | bytes 786440 | tf_op jit(solution)/shard_map/ppermute | solution.py:134
  57.2 0.6 collective-permute-start.2
  57.8 0.2 fusion
  58.0 6.9 %collective-permute-done.refs_1_ = bf16[32,16,256]{2,1,0:T(8,128)(2,1)S(1)} collective-permute-done((bf16[32,16,256]{2,1,0:T(8,128)(2,1)S(1)}, bf16[32,16,256]{2,1,0:T(8,128)(2,1)S(1)}, u32[]{:S(2)}, u32[]{:S(2)}) %collective-permute-start) | collective-permute-done | bytes 262176 | tf_op jit(solution)/shard_map/ppermute | solution.py:134
  64.9 1.1 %collective-permute-start.6 = (bf16[8,16,256]{2,1,0:T(8,128)(2,1)S(1)}, bf16[8,16,256]{2,1,0:T(8,128)(2,1)S(1)}, u32[]{:S(2)}, u32[]{:S(2)}) collective-permute-start(bf16[8,16,256]{2,1,0:T(8,128)(2,1)S(1)} %slice.50), channel_id=1, source_target_pairs={{0,131},{1,128},{2,129},{3,130},{128,3},{129,0},{130,1},{131,2},{4... | collective-permute-start | bytes 196616 | tf_op jit(solution)/shard_map/ppermute | solution.py:142
  66.1 0.2 collective-permute-done.3.refs_4_
  66.3 0.6 collective-permute-start.5
  66.9 1.6 %collective-permute-done.2.refs_3_ = bf16[32,16,256]{2,1,0:T(8,128)(2,1)S(1)} collective-permute-done((bf16[32,16,256]{2,1,0:T(8,128)(2,1)S(1)}, bf16[32,16,256]{2,1,0:T(8,128)(2,1)S(1)}, u32[]{:S(2)}, u32[]{:S(2)}) %collective-permute-start.2) | collective-permute-done | bytes 262176 | tf_op jit(solution)/shard_map/ppermute | solution.py:135
  68.6 1.4 %collective-permute-start.7 = (bf16[24,16,256]{2,1,0:T(8,128)(2,1)S(1)}, bf16[24,16,256]{2,1,0:T(8,128)(2,1)S(1)}, u32[]{:S(2)}, u32[]{:S(2)}) collective-permute-start(bf16[24,16,256]{2,1,0:T(8,128)(2,1)S(1)} %slice.51), channel_id=1, source_target_pairs={{0,129},{1,130},{2,131},{3,128},{128,1},{129,2},{130,3},{131,0},{4... | collective-permute-start | bytes 589832 | tf_op jit(solution)/shard_map/ppermute | solution.py:140
  70.0 1.8 %collective-permute-start.4 = (bf16[16,16,256]{2,1,0:T(8,128)(2,1)S(1)}, bf16[16,16,256]{2,1,0:T(8,128)(2,1)S(1)}, u32[]{:S(2)}, u32[]{:S(2)}) collective-permute-start(bf16[16,16,256]{2,1,0:T(8,128)(2,1)S(1)} %slice.48), channel_id=1, source_target_pairs={{0,128},{128,0},{1,129},{129,1},{2,130},{130,2},{3,131},{131,3},{4... | collective-permute-start | bytes 393224 | tf_op jit(solution)/shard_map/ppermute | solution.py:139
  71.8 3.2 %collective-permute-start.1 = (bf16[32,16,256]{2,1,0:T(8,128)(2,1)S(1)}, bf16[32,16,256]{2,1,0:T(8,128)(2,1)S(1)}, u32[]{:S(2)}, u32[]{:S(2)}) collective-permute-start(bf16[32,16,256]{2,1,0:T(8,128)(2,1)S(1)} %collective-permute-done.refs_1_), channel_id=1, source_target_pairs={{0,3},{1,0},{2,1},{3,2},{4,7},{5,4},{6,5},{7,6},{8,11},{9,8},{10,9... | collective-permute-start | bytes 786440 | tf_op jit(solution)/shard_map/ppermute | solution.py:138
  75.0 0.2 fusion.1.normed
  75.3 1.4 %collective-permute-done.4.refs_5_ = bf16[16,16,256]{2,1,0:T(8,128)(2,1)S(1)} collective-permute-done((bf16[16,16,256]{2,1,0:T(8,128)(2,1)S(1)}, bf16[16,16,256]{2,1,0:T(8,128)(2,1)S(1)}, u32[]{:S(2)}, u32[]{:S(2)}) %collective-permute-start.4) | collective-permute-done | bytes 131104 | tf_op jit(solution)/shard_map/ppermute | solution.py:139
  76.7 2.7 %collective-permute-done.8.refs_9_ = bf16[32,16,256]{2,1,0:T(8,128)(2,1)S(1)} collective-permute-done((bf16[32,16,256]{2,1,0:T(8,128)(2,1)S(1)}, bf16[32,16,256]{2,1,0:T(8,128)(2,1)S(1)}, u32[]{:S(2)}, u32[]{:S(2)}) %collective-permute-start.8) | collective-permute-done | bytes 262176 | tf_op jit(solution)/shard_map/ppermute | solution.py:137
  79.3 1.8 %feed_forward.1 = (bf16[32,4,16,256]{3,2,1,0:T(8,128)(2,1)S(1)}, bf16[32,4,16,256]{3,2,1,0:T(8,128)(2,1)S(1)}, bf16[192,256]{1,0:T(8,128)(2,1)S(1)}, bf16[2,8,96,128]{3,2,1,0:T(8,128)(2,1)S(1)}) custom-call(s32[4]{0:T(128)S(1)} %pad_add_fusion.where, bf16[192,2048]{1,0:T(8,128)(2,1)S(1)} %fusion.1.normed, bf16[32,16,256]{2,1,0:T(8,128)(2,1)S(1)} %bitcast.25, ...), custom_call_target="tpu_custom_call" | custom-call | flops 301989888 | bytes 4194304 | tf_op jit(solution)/shard_map/feed_forward/pallas_call | solution.py:145
  81.3 2.0 %own_side.1 = (bf16[32,4,16,256]{3,2,1,0:T(8,128)(2,1)}, bf16[32,4,16,256]{3,2,1,0:T(8,128)(2,1)}, bf16[2,8,96,128]{3,2,1,0:T(8,128)(2,1)S(1)}) custom-call(s32[4]{0:T(128)S(1)} %pad_add_fusion.where, bf16[192,256]{1,0:T(8,128)(2,1)S(1)} %get-tuple-element.10.active, bf16[32,4,16,256]{3,2,1,0:T(8,128)(2,1)S(1)} %get-tuple-element.11.up, ...), custom_call_target="tpu_custom_call" | custom-call | flops 100663296 | bytes 4194304 | tf_op jit(solution)/shard_map/own_side/pallas_call | solution.py:159
  83.4 0.5 collective-permute-start.10
  84.0 2.8 %collective-permute-start.11 = (bf16[4,96,128]{2,1,0:T(8,128)(2,1)S(1)}, bf16[4,96,128]{2,1,0:T(8,128)(2,1)S(1)}, u32[]{:S(2)}, u32[]{:S(2)}) collective-permute-start(bf16[4,96,128]{2,1,0:T(8,128)(2,1)S(1)} %get-tuple-element.18), channel_id=1, source_target_pairs={{0,120},{8,0},{16,8},{24,16},{32,24},{40,32},{48,40},{56,48},{64,5... | collective-permute-start | bytes 294920 | tf_op jit(solution)/shard_map/ppermute | solution.py:175
  86.8 3.1 %collective-permute-done.10 = bf16[4,96,128]{2,1,0:T(8,128)(2,1)S(1)} collective-permute-done((bf16[4,96,128]{2,1,0:T(8,128)(2,1)S(1)}, bf16[4,96,128]{2,1,0:T(8,128)(2,1)S(1)}, u32[]{:S(2)}, u32[]{:S(2)}) %collective-permute-start.10) | collective-permute-done | bytes 98336 | tf_op jit(solution)/shard_map/ppermute | solution.py:174
  90.0 21.1 %all_to_all.17.arrived = bf16[8,96,128]{2,1,0:T(8,128)(2,1)S(1)} all-to-all(bf16[8,96,128]{2,1,0:T(8,128)(2,1)S(1)} %fusion.2), channel_id=1, replica_groups={{112,96,80,64,48,32,16,0},{88,40,120,72,24,104,56,8},{113,97,81,65,49,3..., dimensions={0} | all-to-all | bytes 393216 | tf_op jit(solution)/shard_map/all_to_all | solution.py:180
  111.1 0.7 summed_up.1
  (23 shorter events, 0.7 us)
Async XLA Ops:
  2.1 55.6 %copy-start = (bf16[192,2048]{1,0:T(8,128)(2,1)S(1)}, bf16[192,2048]{1,0:T(8,128)(2,1)}, u32[]{:S(2)}) copy-start(bf16[192,2048]{1,0:T(8,128)(2,1)} %param.4) | copy-start | bytes 2359300
  55.7 9.2 %collective-permute-start = (bf16[32,16,256]{2,1,0:T(8,128)(2,1)S(1)}, bf16[32,16,256]{2,1,0:T(8,128)(2,1)S(1)}, u32[]{:S(2)}, u32[]{:S(2)}) collective-permute-start(bf16[32,16,256]{2,1,0:T(8,128)(2,1)S(1)} %bitcast.22), channel_id=1, source_target_pairs={{0,3},{1,0},{2,1},{3,2},{4,7},{5,4},{6,5},{7,6},{8,11},{9,8},{10,9... | collective-permute-start | bytes 786440 | tf_op jit(solution)/shard_map/ppermute | solution.py:134
  57.2 9.1 %collective-permute-start.3 = (bf16[32,16,256]{2,1,0:T(8,128)(2,1)S(1)}, bf16[32,16,256]{2,1,0:T(8,128)(2,1)S(1)}, u32[]{:S(2)}, u32[]{:S(2)}) collective-permute-start(bf16[32,16,256]{2,1,0:T(8,128)(2,1)S(1)} %bitcast.23), channel_id=1, source_target_pairs={{0,128},{128,0},{1,129},{129,1},{2,130},{130,2},{3,131},{131,3},{4... | collective-permute-start | bytes 786440 | tf_op jit(solution)/shard_map/ppermute | solution.py:133
  57.2 11.3 %collective-permute-start.2 = (bf16[32,16,256]{2,1,0:T(8,128)(2,1)S(1)}, bf16[32,16,256]{2,1,0:T(8,128)(2,1)S(1)}, u32[]{:S(2)}, u32[]{:S(2)}) collective-permute-start(bf16[32,16,256]{2,1,0:T(8,128)(2,1)S(1)} %bitcast.24), channel_id=1, source_target_pairs={{0,1},{1,2},{2,3},{3,0},{4,5},{5,6},{6,7},{7,4},{8,9},{9,10},{10,1... | collective-permute-start | bytes 786440 | tf_op jit(solution)/shard_map/ppermute | solution.py:135
  64.9 6.8 %collective-permute-start.6 = (bf16[8,16,256]{2,1,0:T(8,128)(2,1)S(1)}, bf16[8,16,256]{2,1,0:T(8,128)(2,1)S(1)}, u32[]{:S(2)}, u32[]{:S(2)}) collective-permute-start(bf16[8,16,256]{2,1,0:T(8,128)(2,1)S(1)} %slice.50), channel_id=1, source_target_pairs={{0,131},{1,128},{2,129},{3,130},{128,3},{129,0},{130,1},{131,2},{4... | collective-permute-start | bytes 196616 | tf_op jit(solution)/shard_map/ppermute | solution.py:142
  66.3 9.0 %collective-permute-start.5 = (bf16[16,16,256]{2,1,0:T(8,128)(2,1)S(1)}, bf16[16,16,256]{2,1,0:T(8,128)(2,1)S(1)}, u32[]{:S(2)}, u32[]{:S(2)}) collective-permute-start(bf16[16,16,256]{2,1,0:T(8,128)(2,1)S(1)} %slice.49), channel_id=1, source_target_pairs={{0,3},{1,0},{2,1},{3,2},{4,7},{5,4},{6,5},{7,6},{8,11},{9,8},{10,9... | collective-permute-start | bytes 393224 | tf_op jit(solution)/shard_map/ppermute | solution.py:141
  68.6 8.1 %collective-permute-start.7 = (bf16[24,16,256]{2,1,0:T(8,128)(2,1)S(1)}, bf16[24,16,256]{2,1,0:T(8,128)(2,1)S(1)}, u32[]{:S(2)}, u32[]{:S(2)}) collective-permute-start(bf16[24,16,256]{2,1,0:T(8,128)(2,1)S(1)} %slice.51), channel_id=1, source_target_pairs={{0,129},{1,130},{2,131},{3,128},{128,1},{129,2},{130,3},{131,0},{4... | collective-permute-start | bytes 589832 | tf_op jit(solution)/shard_map/ppermute | solution.py:140
  70.0 6.7 %collective-permute-start.4 = (bf16[16,16,256]{2,1,0:T(8,128)(2,1)S(1)}, bf16[16,16,256]{2,1,0:T(8,128)(2,1)S(1)}, u32[]{:S(2)}, u32[]{:S(2)}) collective-permute-start(bf16[16,16,256]{2,1,0:T(8,128)(2,1)S(1)} %slice.48), channel_id=1, source_target_pairs={{0,128},{128,0},{1,129},{129,1},{2,130},{130,2},{3,131},{131,3},{4... | collective-permute-start | bytes 393224 | tf_op jit(solution)/shard_map/ppermute | solution.py:139
  71.8 7.6 %collective-permute-start.8 = (bf16[32,16,256]{2,1,0:T(8,128)(2,1)S(1)}, bf16[32,16,256]{2,1,0:T(8,128)(2,1)S(1)}, u32[]{:S(2)}, u32[]{:S(2)}) collective-permute-start(bf16[32,16,256]{2,1,0:T(8,128)(2,1)S(1)} %collective-permute-done.3.refs_4_), channel_id=1, source_target_pairs={{0,1},{1,2},{2,3},{3,0},{4,5},{5,6},{6,7},{7,4},{8,9},{9,10},{10,1... | collective-permute-start | bytes 786440 | tf_op jit(solution)/shard_map/ppermute | solution.py:137
  71.8 7.6 %collective-permute-start.1 = (bf16[32,16,256]{2,1,0:T(8,128)(2,1)S(1)}, bf16[32,16,256]{2,1,0:T(8,128)(2,1)S(1)}, u32[]{:S(2)}, u32[]{:S(2)}) collective-permute-start(bf16[32,16,256]{2,1,0:T(8,128)(2,1)S(1)} %collective-permute-done.refs_1_), channel_id=1, source_target_pairs={{0,3},{1,0},{2,1},{3,2},{4,7},{5,4},{6,5},{7,6},{8,11},{9,8},{10,9... | collective-permute-start | bytes 786440 | tf_op jit(solution)/shard_map/ppermute | solution.py:138
  81.2 2.2 %collective-permute-start.9 = (bf16[2,8,96,128]{3,2,1,0:T(8,128)(2,1)S(1)}, bf16[2,8,96,128]{3,2,1,0:T(8,128)(2,1)S(1)}, u32[]{:S(2)}, u32[]{:S(2)}) collective-permute-start(bf16[2,8,96,128]{3,2,1,0:T(8,128)(2,1)S(1)} %get-tuple-element.16), channel_id=1, source_target_pairs={{0,4},{4,0},{1,5},{5,1},{2,6},{6,2},{3,7},{7,3},{8,12},{12,8},{9,1... | collective-permute-start | bytes 1179656 | tf_op jit(solution)/shard_map/ppermute | solution.py:171
  83.4 6.5 %collective-permute-start.10 = (bf16[4,96,128]{2,1,0:T(8,128)(2,1)S(1)}, bf16[4,96,128]{2,1,0:T(8,128)(2,1)S(1)}, u32[]{:S(2)}, u32[]{:S(2)}) collective-permute-start(bf16[4,96,128]{2,1,0:T(8,128)(2,1)S(1)} %get-tuple-element.17), channel_id=1, source_target_pairs={{0,8},{8,16},{16,24},{24,32},{32,40},{40,48},{48,56},{56,64},{64,7... | collective-permute-start | bytes 294920 | tf_op jit(solution)/shard_map/ppermute | solution.py:174
  84.0 6.0 %collective-permute-start.11 = (bf16[4,96,128]{2,1,0:T(8,128)(2,1)S(1)}, bf16[4,96,128]{2,1,0:T(8,128)(2,1)S(1)}, u32[]{:S(2)}, u32[]{:S(2)}) collective-permute-start(bf16[4,96,128]{2,1,0:T(8,128)(2,1)S(1)} %get-tuple-element.18), channel_id=1, source_target_pairs={{0,120},{8,0},{16,8},{24,16},{32,24},{40,32},{48,40},{56,48},{64,5... | collective-permute-start | bytes 294920 | tf_op jit(solution)/shard_map/ppermute | solution.py:175

commit v5 on v4

--- a/solution.py
+++ b/solution.py
@@ -34,13 +34,14 @@
     return [(blocks - 1 - (3 if odd else 1) * block) % blocks for block in range(blocks)]
 
 
-def partial_sums(out, parity, side, cores, active, down):
+def partial_sums(out, parity, side, cores, active, down, parts=(1, 0)):
     shards, groups, quarter, width = down.shape
     rows, blocks = groups * quarter, shards // cores // 2
     head, tail = active[:LANES], active[LANES:]
     none = jnp.zeros_like(tail)
     upper, lower = jnp.concatenate([tail, none]), jnp.concatenate([none, tail])
-    for part in (1, 0):
+    for at, part in enumerate(parts):
+        at = part if len(parts) > 1 else at
         on = lax.rem(parity + part, 2) * cores + side
         weights = down.reshape(blocks, 2 * cores, rows, width)[:, pl.ds(on, 1)][:, 0]
         wide = nt_dot(weights.reshape(blocks * rows, width), head).astype(out.dtype).reshape(blocks, rows, LANES)
@@ -51,8 +52,8 @@
         odd = lax.rem(parity + part, 2)
         for block, (even_place, odd_place) in enumerate(zip(places(blocks, False), places(blocks, True))):
             place = pl.ds(jnp.where(odd == 0, even_place, odd_place), 1)
-            out[part, place, :rows] = wide[block][None]
-            out[part, place, rows:] = packed[block][None]
+            out[at, place, :rows] = wide[block][None]
+            out[at, place, rows:] = packed[block][None]
 
 
 def feed_forward(cores, where, normed, *refs):
@@ -88,9 +89,13 @@
     writes = [pltpu.make_async_copy(up, up_out, sems.at[0]), pltpu.make_async_copy(down, down_out, sems.at[1])]
     for write in writes:
         write.start()
-    partial_sums(kept, where[3], where[1], cores, active[...], down)
+    partial_sums(kept, where[3], where[1], cores, active[...], down, (0,))
     for write in writes:
         write.wait()
+
+
+def leaving_side(cores, where, active, down, kept):
+    partial_sums(kept, where[3], where[1], cores, active[...], down, (1,))
 
 
 def added(a, b):
@@ -156,9 +161,21 @@
         where, normed, own, left, far, right,
         twin, twin_left_first, twin_left_second, twin_far_first, twin_far_second, twin_right,
     )
+    one = jax.ShapeDtypeStruct((1, *part.shape[1:]), jnp.bfloat16)
+    kept_leaving = pl.pallas_call(
+        functools.partial(leaving_side, cores),
+        out_shape=one,
+        in_specs=[smem] + [vmem] * 2,
+        out_specs=vmem,
+        compiler_params=pltpu.CompilerParams(vmem_limit_bytes=16 << 20),
+        cost_estimate=pl.CostEstimate(
+            flops=count * features * width // 2, bytes_accessed=2 * features * width, transcendentals=0
+        ),
+        name="leaving_side",
+    )(where, active, down)
     up_serving, down_serving, kept = pl.pallas_call(
         functools.partial(own_side, cores),
-        out_shape=[served, served, part],
+        out_shape=[served, served, one],
         in_specs=[smem] + [vmem] * 3,
         out_specs=[pl.BlockSpec(memory_space=pl.ANY)] * 2 + [vmem],
         scratch_shapes=[pltpu.SemaphoreType.DMA((2,))],
@@ -169,7 +186,7 @@
         name="own_side",
     )(where, active, up, down)
     swapped = lax.ppermute(away, "core", ring(cores, 1))
-    leaving = added(kept[1], swapped[1])
+    leaving = added(kept_leaving[0], swapped[1])
     mid = chips // 4
     up_one = lax.ppermute(leaving[:mid], "z", ring(chips, 1))
     down_one = lax.ppermute(leaving[mid:], "z", ring(chips, -1))

time: 113 us -> 111 us (0.982)
  waiting for transfers between devices: 16 us -> 14.6 us
    ppermute x1, waiting for transfers between devices: 3.14 us -> 0.91 us  [local(): up_one = lax.ppermute(leaving[:mid], 'z', ring(chips, 1))]
  transfers between devices with their start and end apart: 12 -> 12, of which waited for: 6 -> 7; matrix products, arithmetic and copies ran while one was open for 0% -> 1% of each run, Pallas kernels for 2% -> 2%
where the time goes in v5:
time: 111 us
  blocking collectives  74.2 us (67%)
  waiting for transfers between devices  14.6 us (13%)
  starting transfers between devices  13.7 us (12%)
  Pallas kernels  5.26 us (5%)
  other arithmetic  1.97 us (2%)
    all_to_all x1, blocking collectives, local(): lax.all_to_all(moved, 'z', 0, 0, tiled=True).reshape(shards, quarter, width)  42.1 us
    all_to_all x1, blocking collectives, local(): lax.all_to_all(summed, 'z', 0, 0, axis_index_groups=same_parity, tiled=True)  20.7 us
    all_to_all x1, blocking collectives, local(): moved = lax.all_to_all(pieces, ('core', 'tp'), 0, 0, tiled=True)  11.4 us
    ppermute x1, waiting for transfers between devices, local(): left = lax.ppermute(own, 'tp', ring(groups, -1))  6.94 us
    ppermute x1, starting transfers between devices, local(): far = lax.ppermute(left, 'tp', ring(groups, -1))  3.23 us
    ppermute x1, starting transfers between devices, local(): down_one = lax.ppermute(leaving[mid:], 'z', ring(chips, -1))  2.84 us
    ppermute x1, waiting for transfers between devices, local(): twin_right = lax.ppermute(twin, 'tp', ring(groups, 1))  2.68 us
  transfers between devices with their start and end apart: 12, of which 7 were waited for; matrix products, arithmetic and copies ran while one was open for 1% of the time, Pallas kernels for 2%

profile of v5, /device:TPU:40, one launch (start us, length us, event | category | flops | bytes accessed | tf_op | source)
XLA Modules:
  0.0 110.8 jit_solution(11821194418282195417)
XLA Ops:
  0.6 1.3 %select_convert_fusion = bf16[64,2048]{1,0:T(8,128)(2,1)S(1)} fusion(f32[64,2048]{1,0:T(8,128)} %param.7, f32[64,2048]{1,0:T(8,128)} %param.6, f32[64]{0:T(128)} %param.5, pred[]{:T(512)S(6)} %eq.5), kind=kLoop, calls=%fused_computation.4 | loop fusion | flops 262144 | bytes 1310977 | tf_op jit(solution)/shard_map/convert_element_type | solution.py:128
  2.2 11.4 %all_to_all.15 = bf16[8,4,16,256]{3,2,1,0:T(8,128)(2,1)S(1)} all-to-all(bf16[8,4,16,256]{3,2,1,0:T(8,128)(2,1)S(1)} %bitcast.27), channel_id=1, replica_groups=mesh['pair'=1,'member'=2,'z'=16,'core'=2,'tp'=4] {'core','tp'}, dimensions={0} | all-to-all | bytes 524288 | tf_op jit(solution)/shard_map/all_to_all | solution.py:131
  13.6 42.1 %all_to_all.16 = bf16[16,2,16,256]{3,2,1,0:T(8,128)(2,1)S(1)} all-to-all(bf16[16,2,16,256]{3,2,1,0:T(8,128)(2,1)S(1)} %copy.11), channel_id=1, replica_groups=mesh['pair'=1,'member'=2,'z'=16,'core'=2,'tp'=4] {'z'}, dimensions={0} | all-to-all | bytes 524288 | tf_op jit(solution)/shard_map/all_to_all | solution.py:133
  55.7 1.5 %collective-permute-start = (bf16[32,16,256]{2,1,0:T(8,128)(2,1)S(1)}, bf16[32,16,256]{2,1,0:T(8,128)(2,1)S(1)}, u32[]{:S(2)}, u32[]{:S(2)}) collective-permute-start(bf16[32,16,256]{2,1,0:T(8,128)(2,1)S(1)} %bitcast.22), channel_id=1, source_target_pairs={{0,3},{1,0},{2,1},{3,2},{4,7},{5,4},{6,5},{7,6},{8,11},{9,8},{10,9... | collective-permute-start | bytes 786440 | tf_op jit(solution)/shard_map/ppermute | solution.py:139
  57.2 0.6 collective-permute-start.2
  57.8 0.2 fusion
  58.0 6.9 %collective-permute-done.refs_1_ = bf16[32,16,256]{2,1,0:T(8,128)(2,1)S(1)} collective-permute-done((bf16[32,16,256]{2,1,0:T(8,128)(2,1)S(1)}, bf16[32,16,256]{2,1,0:T(8,128)(2,1)S(1)}, u32[]{:S(2)}, u32[]{:S(2)}) %collective-permute-start) | collective-permute-done | bytes 262176 | tf_op jit(solution)/shard_map/ppermute | solution.py:139
  64.9 1.1 %collective-permute-start.6 = (bf16[8,16,256]{2,1,0:T(8,128)(2,1)S(1)}, bf16[8,16,256]{2,1,0:T(8,128)(2,1)S(1)}, u32[]{:S(2)}, u32[]{:S(2)}) collective-permute-start(bf16[8,16,256]{2,1,0:T(8,128)(2,1)S(1)} %slice.42), channel_id=1, source_target_pairs={{0,131},{1,128},{2,129},{3,130},{128,3},{129,0},{130,1},{131,2},{4... | collective-permute-start | bytes 196616 | tf_op jit(solution)/shard_map/ppermute | solution.py:147
  66.3 0.6 collective-permute-start.5
  66.9 1.6 %collective-permute-done.2.refs_3_ = bf16[32,16,256]{2,1,0:T(8,128)(2,1)S(1)} collective-permute-done((bf16[32,16,256]{2,1,0:T(8,128)(2,1)S(1)}, bf16[32,16,256]{2,1,0:T(8,128)(2,1)S(1)}, u32[]{:S(2)}, u32[]{:S(2)}) %collective-permute-start.2) | collective-permute-done | bytes 262176 | tf_op jit(solution)/shard_map/ppermute | solution.py:140
  68.6 1.4 %collective-permute-start.7 = (bf16[24,16,256]{2,1,0:T(8,128)(2,1)S(1)}, bf16[24,16,256]{2,1,0:T(8,128)(2,1)S(1)}, u32[]{:S(2)}, u32[]{:S(2)}) collective-permute-start(bf16[24,16,256]{2,1,0:T(8,128)(2,1)S(1)} %slice.43), channel_id=1, source_target_pairs={{0,129},{1,130},{2,131},{3,128},{128,1},{129,2},{130,3},{131,0},{4... | collective-permute-start | bytes 589832 | tf_op jit(solution)/shard_map/ppermute | solution.py:145
  70.0 1.8 %collective-permute-start.4 = (bf16[16,16,256]{2,1,0:T(8,128)(2,1)S(1)}, bf16[16,16,256]{2,1,0:T(8,128)(2,1)S(1)}, u32[]{:S(2)}, u32[]{:S(2)}) collective-permute-start(bf16[16,16,256]{2,1,0:T(8,128)(2,1)S(1)} %slice.40), channel_id=1, source_target_pairs={{0,128},{128,0},{1,129},{129,1},{2,130},{130,2},{3,131},{131,3},{4... | collective-permute-start | bytes 393224 | tf_op jit(solution)/shard_map/ppermute | solution.py:144
  71.8 3.2 %collective-permute-start.1 = (bf16[32,16,256]{2,1,0:T(8,128)(2,1)S(1)}, bf16[32,16,256]{2,1,0:T(8,128)(2,1)S(1)}, u32[]{:S(2)}, u32[]{:S(2)}) collective-permute-start(bf16[32,16,256]{2,1,0:T(8,128)(2,1)S(1)} %collective-permute-done.refs_1_), channel_id=1, source_target_pairs={{0,3},{1,0},{2,1},{3,2},{4,7},{5,4},{6,5},{7,6},{8,11},{9,8},{10,9... | collective-permute-start | bytes 786440 | tf_op jit(solution)/shard_map/ppermute | solution.py:143
  75.3 1.4 %collective-permute-done.4.refs_5_ = bf16[16,16,256]{2,1,0:T(8,128)(2,1)S(1)} collective-permute-done((bf16[16,16,256]{2,1,0:T(8,128)(2,1)S(1)}, bf16[16,16,256]{2,1,0:T(8,128)(2,1)S(1)}, u32[]{:S(2)}, u32[]{:S(2)}) %collective-permute-start.4) | collective-permute-done | bytes 131104 | tf_op jit(solution)/shard_map/ppermute | solution.py:144
  76.7 2.7 %collective-permute-done.8.refs_9_ = bf16[32,16,256]{2,1,0:T(8,128)(2,1)S(1)} collective-permute-done((bf16[32,16,256]{2,1,0:T(8,128)(2,1)S(1)}, bf16[32,16,256]{2,1,0:T(8,128)(2,1)S(1)}, u32[]{:S(2)}, u32[]{:S(2)}) %collective-permute-start.8) | collective-permute-done | bytes 262176 | tf_op jit(solution)/shard_map/ppermute | solution.py:142
  79.3 1.8 %feed_forward.1 = (bf16[32,4,16,256]{3,2,1,0:T(8,128)(2,1)S(1)}, bf16[32,4,16,256]{3,2,1,0:T(8,128)(2,1)S(1)}, bf16[192,256]{1,0:T(8,128)(2,1)S(1)}, bf16[2,8,96,128]{3,2,1,0:T(8,128)(2,1)S(1)}) custom-call(s32[4]{0:T(128)S(1)} %pad_add_fusion.where, bf16[192,2048]{1,0:T(8,128)(2,1)S(1)} %fusion.1.normed, bf16[32,16,256]{2,1,0:T(8,128)(2,1)S(1)} %bitcast.25, ...), custom_call_target="tpu_custom_call" | custom-call | flops 301989888 | bytes 4194304 | tf_op jit(solution)/shard_map/feed_forward/pallas_call | solution.py:150
  81.3 0.8 leaving_side.1
  82.2 0.9 collective-permute-done.9
  83.1 0.5 collective-permute-start.10
  83.6 2.8 %collective-permute-start.11 = (bf16[4,96,128]{2,1,0:T(8,128)(2,1)S(1)}, bf16[4,96,128]{2,1,0:T(8,128)(2,1)S(1)}, u32[]{:S(2)}, u32[]{:S(2)}) collective-permute-start(bf16[4,96,128]{2,1,0:T(8,128)(2,1)S(1)} %get-tuple-element.18), channel_id=1, source_target_pairs={{0,120},{8,0},{16,8},{24,16},{32,24},{40,32},{48,40},{56,48},{64,5... | collective-permute-start | bytes 294920 | tf_op jit(solution)/shard_map/ppermute | solution.py:192
  86.5 1.9 %own_side.1 = (bf16[32,4,16,256]{3,2,1,0:T(8,128)(2,1)}, bf16[32,4,16,256]{3,2,1,0:T(8,128)(2,1)}, bf16[1,8,96,128]{3,2,1,0:T(8,128)(2,1)S(1)}) custom-call(s32[4]{0:T(128)S(1)} %pad_add_fusion.where, bf16[192,256]{1,0:T(8,128)(2,1)S(1)} %get-tuple-element.10.active, bf16[32,4,16,256]{3,2,1,0:T(8,128)(2,1)S(1)} %get-tuple-element.11.up, ...), custom_call_target="tpu_custom_call" | custom-call | flops 100663296 | bytes 4194304 | tf_op jit(solution)/shard_map/own_side/pallas_call | solution.py:176
  88.4 0.9 collective-permute-done.10
  89.4 20.7 %all_to_all.17.arrived = bf16[8,96,128]{2,1,0:T(8,128)(2,1)S(1)} all-to-all(bf16[8,96,128]{2,1,0:T(8,128)(2,1)S(1)} %fusion.2), channel_id=1, replica_groups={{112,96,80,64,48,32,16,0},{88,40,120,72,24,104,56,8},{113,97,81,65,49,3..., dimensions={0} | all-to-all | bytes 393216 | tf_op jit(solution)/shard_map/all_to_all | solution.py:197
  110.1 0.7 summed_up.1
  (24 shorter events, 1.1 us)
Async XLA Ops:
  2.1 55.6 %copy-start = (bf16[192,2048]{1,0:T(8,128)(2,1)S(1)}, bf16[192,2048]{1,0:T(8,128)(2,1)}, u32[]{:S(2)}) copy-start(bf16[192,2048]{1,0:T(8,128)(2,1)} %param.4) | copy-start | bytes 2359300
  55.7 9.2 %collective-permute-start = (bf16[32,16,256]{2,1,0:T(8,128)(2,1)S(1)}, bf16[32,16,256]{2,1,0:T(8,128)(2,1)S(1)}, u32[]{:S(2)}, u32[]{:S(2)}) collective-permute-start(bf16[32,16,256]{2,1,0:T(8,128)(2,1)S(1)} %bitcast.22), channel_id=1, source_target_pairs={{0,3},{1,0},{2,1},{3,2},{4,7},{5,4},{6,5},{7,6},{8,11},{9,8},{10,9... | collective-permute-start | bytes 786440 | tf_op jit(solution)/shard_map/ppermute | solution.py:139
  57.2 9.1 %collective-permute-start.3 = (bf16[32,16,256]{2,1,0:T(8,128)(2,1)S(1)}, bf16[32,16,256]{2,1,0:T(8,128)(2,1)S(1)}, u32[]{:S(2)}, u32[]{:S(2)}) collective-permute-start(bf16[32,16,256]{2,1,0:T(8,128)(2,1)S(1)} %bitcast.23), channel_id=1, source_target_pairs={{0,128},{128,0},{1,129},{129,1},{2,130},{130,2},{3,131},{131,3},{4... | collective-permute-start | bytes 786440 | tf_op jit(solution)/shard_map/ppermute | solution.py:138
  57.2 11.3 %collective-permute-start.2 = (bf16[32,16,256]{2,1,0:T(8,128)(2,1)S(1)}, bf16[32,16,256]{2,1,0:T(8,128)(2,1)S(1)}, u32[]{:S(2)}, u32[]{:S(2)}) collective-permute-start(bf16[32,16,256]{2,1,0:T(8,128)(2,1)S(1)} %bitcast.24), channel_id=1, source_target_pairs={{0,1},{1,2},{2,3},{3,0},{4,5},{5,6},{6,7},{7,4},{8,9},{9,10},{10,1... | collective-permute-start | bytes 786440 | tf_op jit(solution)/shard_map/ppermute | solution.py:140
  64.9 6.8 %collective-permute-start.6 = (bf16[8,16,256]{2,1,0:T(8,128)(2,1)S(1)}, bf16[8,16,256]{2,1,0:T(8,128)(2,1)S(1)}, u32[]{:S(2)}, u32[]{:S(2)}) collective-permute-start(bf16[8,16,256]{2,1,0:T(8,128)(2,1)S(1)} %slice.42), channel_id=1, source_target_pairs={{0,131},{1,128},{2,129},{3,130},{128,3},{129,0},{130,1},{131,2},{4... | collective-permute-start | bytes 196616 | tf_op jit(solution)/shard_map/ppermute | solution.py:147
  66.3 9.0 %collective-permute-start.5 = (bf16[16,16,256]{2,1,0:T(8,128)(2,1)S(1)}, bf16[16,16,256]{2,1,0:T(8,128)(2,1)S(1)}, u32[]{:S(2)}, u32[]{:S(2)}) collective-permute-start(bf16[16,16,256]{2,1,0:T(8,128)(2,1)S(1)} %slice.41), channel_id=1, source_target_pairs={{0,3},{1,0},{2,1},{3,2},{4,7},{5,4},{6,5},{7,6},{8,11},{9,8},{10,9... | collective-permute-start | bytes 393224 | tf_op jit(solution)/shard_map/ppermute | solution.py:146
  68.6 8.1 %collective-permute-start.7 = (bf16[24,16,256]{2,1,0:T(8,128)(2,1)S(1)}, bf16[24,16,256]{2,1,0:T(8,128)(2,1)S(1)}, u32[]{:S(2)}, u32[]{:S(2)}) collective-permute-start(bf16[24,16,256]{2,1,0:T(8,128)(2,1)S(1)} %slice.43), channel_id=1, source_target_pairs={{0,129},{1,130},{2,131},{3,128},{128,1},{129,2},{130,3},{131,0},{4... | collective-permute-start | bytes 589832 | tf_op jit(solution)/shard_map/ppermute | solution.py:145
  70.0 6.7 %collective-permute-start.4 = (bf16[16,16,256]{2,1,0:T(8,128)(2,1)S(1)}, bf16[16,16,256]{2,1,0:T(8,128)(2,1)S(1)}, u32[]{:S(2)}, u32[]{:S(2)}) collective-permute-start(bf16[16,16,256]{2,1,0:T(8,128)(2,1)S(1)} %slice.40), channel_id=1, source_target_pairs={{0,128},{128,0},{1,129},{129,1},{2,130},{130,2},{3,131},{131,3},{4... | collective-permute-start | bytes 393224 | tf_op jit(solution)/shard_map/ppermute | solution.py:144
  71.8 7.6 %collective-permute-start.8 = (bf16[32,16,256]{2,1,0:T(8,128)(2,1)S(1)}, bf16[32,16,256]{2,1,0:T(8,128)(2,1)S(1)}, u32[]{:S(2)}, u32[]{:S(2)}) collective-permute-start(bf16[32,16,256]{2,1,0:T(8,128)(2,1)S(1)} %collective-permute-done.3.refs_4_), channel_id=1, source_target_pairs={{0,1},{1,2},{2,3},{3,0},{4,5},{5,6},{6,7},{7,4},{8,9},{9,10},{10,1... | collective-permute-start | bytes 786440 | tf_op jit(solution)/shard_map/ppermute | solution.py:142
  71.8 7.6 %collective-permute-start.1 = (bf16[32,16,256]{2,1,0:T(8,128)(2,1)S(1)}, bf16[32,16,256]{2,1,0:T(8,128)(2,1)S(1)}, u32[]{:S(2)}, u32[]{:S(2)}) collective-permute-start(bf16[32,16,256]{2,1,0:T(8,128)(2,1)S(1)} %collective-permute-done.refs_1_), channel_id=1, source_target_pairs={{0,3},{1,0},{2,1},{3,2},{4,7},{5,4},{6,5},{7,6},{8,11},{9,8},{10,9... | collective-permute-start | bytes 786440 | tf_op jit(solution)/shard_map/ppermute | solution.py:143
  81.2 1.8 %collective-permute-start.9 = (bf16[2,8,96,128]{3,2,1,0:T(8,128)(2,1)S(1)}, bf16[2,8,96,128]{3,2,1,0:T(8,128)(2,1)S(1)}, u32[]{:S(2)}, u32[]{:S(2)}) collective-permute-start(bf16[2,8,96,128]{3,2,1,0:T(8,128)(2,1)S(1)} %get-tuple-element.16), channel_id=1, source_target_pairs={{0,4},{4,0},{1,5},{5,1},{2,6},{6,2},{3,7},{7,3},{8,12},{12,8},{9,1... | collective-permute-start | bytes 1179656 | tf_op jit(solution)/shard_map/ppermute | solution.py:188
  83.1 6.2 %collective-permute-start.10 = (bf16[4,96,128]{2,1,0:T(8,128)(2,1)S(1)}, bf16[4,96,128]{2,1,0:T(8,128)(2,1)S(1)}, u32[]{:S(2)}, u32[]{:S(2)}) collective-permute-start(bf16[4,96,128]{2,1,0:T(8,128)(2,1)S(1)} %get-tuple-element.17), channel_id=1, source_target_pairs={{0,8},{8,16},{16,24},{24,32},{32,40},{40,48},{48,56},{56,64},{64,7... | collective-permute-start | bytes 294920 | tf_op jit(solution)/shard_map/ppermute | solution.py:191
  83.6 5.7 %collective-permute-start.11 = (bf16[4,96,128]{2,1,0:T(8,128)(2,1)S(1)}, bf16[4,96,128]{2,1,0:T(8,128)(2,1)S(1)}, u32[]{:S(2)}, u32[]{:S(2)}) collective-permute-start(bf16[4,96,128]{2,1,0:T(8,128)(2,1)S(1)} %get-tuple-element.18), channel_id=1, source_target_pairs={{0,120},{8,0},{16,8},{24,16},{32,24},{40,32},{48,40},{56,48},{64,5... | collective-permute-start | bytes 294920 | tf_op jit(solution)/shard_map/ppermute | solution.py:192
